TPU v7x, 32 devices: a whole 2x2x4 slice. The times are simulated.
32 devices in a mesh: ep: 8 (over z, x), tp: 4 (over y, core).
Axes of the slice: x: 2, y: 2, z: 4, core: 2. Of those that a mesh axis runs over, the one named last changes fastest.
Arguments:
- tokens: bfloat16 [1024, 2048], P('ep', 'tp'), may hold values from -20 to 20
- routing: int32 [1024, 2], P('ep'), may hold values from 0 to 7, all different within a row; in each aligned block of 128 rows (0 to 127, 128 to 255, ...) at most 48 rows name the same one
- gate_weights: bfloat16 [1024, 2], P('ep'), may hold values from 0 to 1, as said below
- cotangent: bfloat16 [1024, 2048], P('ep', 'tp'), may hold values from -3 to 3
- expert_gate: bfloat16 [8, 2048, 3072], P('ep', None, 'tp'), may hold values from -3 to 3
- expert_up: bfloat16 [8, 2048, 3072], P('ep', None, 'tp'), may hold values from -3 to 3
- expert_down: bfloat16 [8, 3072, 2048], P('ep', 'tp'), may hold values from -0.109375 to 0.109375
- router: bfloat16 [2048, 8], replicated, may hold values from -0.125 to 0.125
Outputs:
- token_grad: float32 [1024, 2048], P('ep', 'tp')
- gate_grad: float32 [1024, 2], P('ep')
- gate_proj_grad: bfloat16 [8, 2048, 3072], P('ep', None, 'tp')
- up_proj_grad: bfloat16 [8, 2048, 3072], P('ep', None, 'tp')
- down_proj_grad: bfloat16 [8, 3072, 2048], P('ep', 'tp')
- router_grad: float32 [8, 2048], P('ep', 'tp')
- gate_row_square: float32 [8, 2048], P('ep')
- up_row_square: float32 [8, 2048], P('ep')
- down_row_square: float32 [8, 3072], P('ep', 'tp')
Inputs may be any that keep to these rules, and one draw needn't show every extreme that they name: `routing`: each token names 2 different experts. Among the 128 rows of one device no expert is named more than 48 times; some device reaches 48. `gate_weights`: each row is positive and sums to one up to rounding.
All inputs are finite; a program needn't handle non-finite values.
Results may differ from a plain program's by a relative error of at most 0.015.
Values may be sent and summed in bfloat16 or wider, within the bound.
A program may use at most 64 MiB of HBM per device.

v0:
```python
import functools

import jax
import jax.numpy as jnp
from jax import lax
from jax.experimental import pallas as pl
from jax.experimental.pallas import tpu as pltpu
from jax.sharding import PartitionSpec as P

MESH = pl.DeviceIdType.MESH
F32 = jnp.float32
BF16 = jnp.bfloat16


def matmul_tn(left_side, right_side):
    return lax.dot_general(
        left_side, right_side, (((0,), (0,)), ((), ())), preferred_element_type=F32
    )


def matmul_nt(left_side, right_side):
    return lax.dot_general(
        left_side, right_side, (((1,), (1,)), ((), ())), preferred_element_type=F32
    )


def loop(lower, upper, body):
    if upper - lower <= 8:
        for i in range(lower, upper):
            body(i)
    else:
        lax.fori_loop(lower, upper, lambda i, carry: (body(i), carry)[1], 0)


def place():
    ep, tp = lax.axis_index("ep"), lax.axis_index("tp")
    return ep, tp, lax.div(tp, 2), lax.rem(tp, 2)


def greet(n_ep, n_tp, all_tp, between=None):
    ep, tp, y, core = place()
    barrier = pltpu.get_barrier_semaphore()

    def to_ep(r):
        pl.semaphore_signal(
            barrier, inc=1, device_id=(lax.rem(ep + r, n_ep), tp), device_id_type=MESH
        )

    def to_tp(r):
        pl.semaphore_signal(
            barrier, inc=1, device_id=(ep, lax.rem(tp + r, n_tp)), device_id_type=MESH
        )

    def to_y(r):
        other = lax.rem(y + r, n_tp // 2) * 2 + core
        pl.semaphore_signal(barrier, inc=1, device_id=(ep, other), device_id_type=MESH)

    loop(1, n_ep, to_ep)
    if all_tp:
        loop(1, n_tp, to_tp)
        if between is not None:
            between()
        pl.semaphore_wait(barrier, n_ep - 1 + n_tp - 1)
    else:
        loop(1, n_tp // 2, to_y)
        pl.semaphore_signal(
            barrier, inc=1, device_id=(ep, y * 2 + 1 - core), device_id_type=MESH
        )
        if between is not None:
            between()
        pl.semaphore_wait(barrier, n_ep - 1 + n_tp // 2)


def lane_pick(n_ep, cap, padded):
    shape = (n_ep, cap, padded)
    pick = lax.broadcasted_iota(jnp.int32, shape, 1) == lax.broadcasted_iota(jnp.int32, shape, 2)
    return pick.astype(F32).reshape(n_ep * cap, padded)


def own_block(n_ep, cap):
    shape = (n_ep, n_ep * cap)
    first = lax.broadcasted_iota(jnp.int32, shape, 0) * cap
    slot = lax.broadcasted_iota(jnp.int32, shape, 1)
    return ((slot >= first) & (slot < first + cap)).astype(F32)


def fill_slots(routes_ref, weights_ref, tokens_ref, cotangent_ref, table_ref, x_ref, t_ref, w_ref):
    n_ep, cap, width = x_ref.shape
    top, tok = routes_ref.shape
    padded = w_ref.shape[2]
    routes = routes_ref[...]
    weights = weights_ref[...].astype(F32)
    labels = lax.broadcasted_iota(jnp.int32, (n_ep, tok), 0)
    hit = jnp.zeros((n_ep, tok), F32)
    chosen = jnp.zeros((n_ep, tok), F32)
    for k in range(top):
        same = routes[k : k + 1, :] == labels
        hit = hit + same.astype(F32)
        chosen = chosen + jnp.where(same, weights[k : k + 1, :], 0.0)
    square = (tok, tok)
    before = lax.broadcasted_iota(jnp.int32, square, 0) < lax.broadcasted_iota(jnp.int32, square, 1)
    count = jnp.dot(hit.astype(BF16), before.astype(F32).astype(BF16), preferred_element_type=F32)
    position = jnp.where(hit > 0.0, count, -1.0)
    slot = lax.broadcasted_iota(jnp.int32, (n_ep, cap, tok), 1).astype(F32)
    table = (slot == position[:, None, :]).astype(F32).reshape(n_ep * cap, tok).astype(BF16)
    table_ref[...] = table
    for source, target in ((tokens_ref, x_ref), (cotangent_ref, t_ref)):
        rows = jnp.dot(table, source[...], preferred_element_type=F32)
        target[...] = rows.reshape(n_ep, cap, width).astype(BF16)
    spread = matmul_nt(chosen.astype(BF16), table) * own_block(n_ep, cap)
    values = jnp.dot(
        spread.astype(BF16),
        lane_pick(n_ep, cap, padded).astype(BF16),
        preferred_element_type=F32,
    )
    w_ref[...] = jnp.broadcast_to(values[:, None, :], w_ref.shape)


def dispatch_kernel(
    n_ep,
    n_tp,
    chunks,
    routes_ref,
    weights_ref,
    tokens_ref,
    cotangent_ref,
    ox_ref,
    ot_ref,
    ow_ref,
    table_ref,
    x_ref,
    t_ref,
    w_ref,
    ep_send,
    ep_recv,
    y_send,
    y_recv,
    core_send,
    core_recv,
    own_sem,
):
    ep, tp, y, core = place()
    n_y = n_tp // 2
    width = x_ref.shape[2]
    per = n_ep // chunks
    partner = y * 2 + 1 - core
    fill = functools.partial(
        fill_slots,
        routes_ref,
        weights_ref,
        tokens_ref,
        cotangent_ref,
        table_ref,
        x_ref,
        t_ref,
        w_ref,
    )
    greet(n_ep, n_tp, False, fill)
    sources = (x_ref, t_ref)
    outs = (ox_ref, ot_ref)

    def cols(which):
        return pl.ds(pl.multiple_of(which * width, width), width)

    def ep_copy(which, dst, src):
        if which == 2:
            return pltpu.make_async_remote_copy(
                src_ref=w_ref.at[dst],
                dst_ref=ow_ref.at[src],
                send_sem=ep_send.at[2, dst],
                recv_sem=ep_recv.at[2, src],
                device_id=(dst, tp),
                device_id_type=MESH,
            )
        return pltpu.make_async_remote_copy(
            src_ref=sources[which].at[dst],
            dst_ref=outs[which].at[src, :, cols(tp)],
            send_sem=ep_send.at[which, dst],
            recv_sem=ep_recv.at[which, src],
            device_id=(dst, tp),
            device_id_type=MESH,
        )

    def y_copy(which, source_y, target_y, chunk):
        piece = outs[which].at[pl.ds(chunk * per, per), :, cols(source_y * 2 + core)]
        return pltpu.make_async_remote_copy(
            src_ref=piece,
            dst_ref=piece,
            send_sem=y_send.at[which, target_y, chunk],
            recv_sem=y_recv.at[which, source_y, chunk],
            device_id=(ep, target_y * 2 + core),
            device_id_type=MESH,
        )

    def core_copy(which, source_y, source_core, chunk):
        piece = outs[which].at[pl.ds(chunk * per, per), :, cols(source_y * 2 + source_core)]
        return pltpu.make_async_remote_copy(
            src_ref=piece,
            dst_ref=piece,
            send_sem=core_send.at[which, source_y, chunk],
            recv_sem=core_recv.at[which, source_y, chunk],
            device_id=(ep, partner),
            device_id_type=MESH,
        )

    def own_copy(which):
        if which == 2:
            return pltpu.make_async_copy(w_ref.at[ep], ow_ref.at[ep], own_sem.at[2])
        return pltpu.make_async_copy(
            sources[which].at[ep], outs[which].at[ep, :, cols(tp)], own_sem.at[which]
        )

    for which in range(3):
        own_copy(which).start()

    def send(r):
        for which in range(3):
            ep_copy(which, lax.rem(ep + r, n_ep), ep).start()

    loop(1, n_ep, send)
    for which in range(3):
        own_copy(which).wait()
    my_chunk = lax.div(ep, per)

    def chunk_at(j):
        return lax.rem(my_chunk - j + chunks, chunks)

    def relay(j):
        chunk = chunk_at(j)
        for which in range(2):
            for i in range(per):
                source = chunk * per + i

                @pl.when(source != ep)
                def _():
                    ep_copy(which, ep, source).wait_recv()

            for r in range(1, n_y):
                y_copy(which, y, lax.rem(y + r, n_y), chunk).start()
            core_copy(which, y, core, chunk).start()

    loop(0, chunks, relay)

    def forward(j):
        chunk = chunk_at(j)
        for r in range(1, n_y):
            source_y = lax.rem(y + n_y - r, n_y)
            for which in range(2):
                y_copy(which, source_y, y, chunk).wait_recv()
                core_copy(which, source_y, core, chunk).start()

    loop(0, chunks, forward)

    def finish(j):
        chunk = chunk_at(j)
        for which in range(2):
            for r in range(n_y):
                core_copy(which, r, 1 - core, chunk).wait_recv()
                core_copy(which, r, core, chunk).wait_send()
            for r in range(1, n_y):
                y_copy(which, y, lax.rem(y + r, n_y), chunk).wait_send()

    loop(0, chunks, finish)

    def drain(r):
        other = lax.rem(ep + r, n_ep)
        for which in range(3):
            ep_copy(which, other, ep).wait_send()
        ep_copy(2, ep, other).wait_recv()

    loop(1, n_ep, drain)


def dispatch(routes, weights, tokens, cotangent, n_ep, n_tp, cap):
    tok, width = tokens.shape
    padded = -(-cap // 128) * 128
    chunks = n_ep if n_ep <= 8 else next(c for c in range(8, 0, -1) if n_ep % c == 0)
    n_y = n_tp // 2
    dma = pltpu.SemaphoreType.DMA
    return pl.pallas_call(
        functools.partial(dispatch_kernel, n_ep, n_tp, chunks),
        out_shape=(
            jax.ShapeDtypeStruct((n_ep, cap, width * n_tp), BF16),
            jax.ShapeDtypeStruct((n_ep, cap, width * n_tp), BF16),
            jax.ShapeDtypeStruct((n_ep, 8, padded), F32),
            jax.ShapeDtypeStruct((n_ep * cap, tok), BF16),
        ),
        in_specs=[pl.BlockSpec(memory_space=pltpu.VMEM)] * 4,
        out_specs=[pl.BlockSpec(memory_space=pltpu.VMEM)] * 4,
        scratch_shapes=[
            pltpu.VMEM((n_ep, cap, width), BF16),
            pltpu.VMEM((n_ep, cap, width), BF16),
            pltpu.VMEM((n_ep, 8, padded), F32),
            dma((3, n_ep)),
            dma((3, n_ep)),
            dma((2, n_y, chunks)),
            dma((2, n_y, chunks)),
            dma((2, n_y, chunks)),
            dma((2, n_y, chunks)),
            dma((3,)),
        ],
        compiler_params=pltpu.CompilerParams(collective_id=0, has_side_effects=True),
        name="dispatch",
    )(routes, weights, tokens, cotangent)


def return_kernel(
    n_ep,
    n_tp,
    chunks,
    part_ref,
    gate_ref,
    back_ref,
    back_gate_ref,
    core_buf,
    y_out,
    y_buf,
    ep_out,
    gate_buf,
    gate_out,
    core_send,
    core_recv,
    y_send,
    y_recv,
    ep_send,
    ep_recv,
    tp_send,
    tp_recv,
    gate_send,
    gate_recv,
    own_sem,
):
    ep, tp, y, core = place()
    n_y = n_tp // 2
    width = back_ref.shape[2]
    per = n_ep // chunks
    partner = y * 2 + 1 - core
    greet(n_ep, n_tp, True)

    def cols(which):
        return pl.ds(pl.multiple_of(which * width, width), width)

    def rows(chunk):
        return pl.ds(chunk * per, per)

    def core_copy(target_y, chunk):
        return pltpu.make_async_remote_copy(
            src_ref=part_ref.at[rows(chunk), :, cols(target_y * 2 + 1 - core)],
            dst_ref=core_buf.at[target_y, rows(chunk)],
            send_sem=core_send.at[target_y, chunk],
            recv_sem=core_recv.at[target_y, chunk],
            device_id=(ep, partner),
            device_id_type=MESH,
        )

    def y_copy(source_y, target_y, chunk):
        return pltpu.make_async_remote_copy(
            src_ref=y_out.at[target_y, rows(chunk)],
            dst_ref=y_buf.at[source_y, rows(chunk)],
            send_sem=y_send.at[target_y, chunk],
            recv_sem=y_recv.at[source_y, chunk],
            device_id=(ep, target_y * 2 + core),
            device_id_type=MESH,
        )

    def ep_copy(dst, src):
        return pltpu.make_async_remote_copy(
            src_ref=ep_out.at[dst],
            dst_ref=back_ref.at[src],
            send_sem=ep_send.at[dst],
            recv_sem=ep_recv.at[src],
            device_id=(dst, tp),
            device_id_type=MESH,
        )

    def tp_copy(dst, src):
        return pltpu.make_async_remote_copy(
            src_ref=gate_ref,
            dst_ref=gate_buf.at[src],
            send_sem=tp_send.at[dst],
            recv_sem=tp_recv.at[src],
            device_id=(ep, dst),
            device_id_type=MESH,
        )

    def gate_copy(dst, src):
        return pltpu.make_async_remote_copy(
            src_ref=gate_out.at[dst],
            dst_ref=back_gate_ref.at[src],
            send_sem=gate_send.at[dst],
            recv_sem=gate_recv.at[src],
            device_id=(dst, tp),
            device_id_type=MESH,
        )

    first = lax.div(ep, per)

    def chunk_at(j):
        return lax.rem(first + j, chunks)

    loop(1, n_tp, lambda r: tp_copy(lax.rem(tp + r, n_tp), tp).start())

    def start(j):
        for r in range(n_y):
            core_copy(lax.rem(y + r + 1, n_y), chunk_at(j)).start()

    loop(1, chunks + 1, start)

    def across(j):
        chunk = chunk_at(j)
        for r in range(1, n_y):
            target = lax.rem(y + r, n_y)
            core_copy(target, chunk).wait_recv()
            for i in range(per):
                at = chunk * per + i
                mine = part_ref[at, :, cols(target * 2 + core)].astype(F32)
                y_out[target, at] = (mine + core_buf[target, at].astype(F32)).astype(BF16)
            y_copy(y, target, chunk).start()

    loop(1, chunks + 1, across)

    total = gate_ref[...]
    for r in range(1, n_tp):
        source = lax.rem(tp + r, n_tp)
        tp_copy(tp, source).wait_recv()
        total = total + gate_buf[source]
    gate_out[...] = total
    loop(1, n_ep, lambda r: gate_copy(lax.rem(ep + r, n_ep), ep).start())
    own_gate = pltpu.make_async_copy(gate_out.at[ep], back_gate_ref.at[ep], own_sem.at[0])
    own_gate.start()

    def scatter(j):
        chunk = chunk_at(j)
        core_copy(y, chunk).wait_recv()
        for r in range(1, n_y):
            y_copy(lax.rem(y + r, n_y), y, chunk).wait_recv()
        for i in range(per):
            at = chunk * per + i
            value = part_ref[at, :, cols(tp)].astype(F32) + core_buf[y, at].astype(F32)
            for r in range(1, n_y):
                value = value + y_buf[lax.rem(y + r, n_y), at].astype(F32)
            ep_out[at] = value.astype(BF16)

            @pl.when(at != ep)
            def _():
                ep_copy(at, ep).start()

    loop(1, chunks + 1, scatter)
    own_rows = pltpu.make_async_copy(ep_out.at[ep], back_ref.at[ep], own_sem.at[1])
    own_rows.start()

    def drain(r):
        other = lax.rem(ep + r, n_ep)
        gate_copy(ep, other).wait_recv()
        gate_copy(other, ep).wait_send()
        ep_copy(ep, other).wait_recv()
        ep_copy(other, ep).wait_send()

    loop(1, n_ep, drain)
    loop(1, n_tp, lambda r: tp_copy(lax.rem(tp + r, n_tp), tp).wait_send())

    def finish(chunk):
        for r in range(n_y):
            core_copy(r, chunk).wait_send()
        for r in range(1, n_y):
            y_copy(y, lax.rem(y + r, n_y), chunk).wait_send()

    loop(0, chunks, finish)
    own_gate.wait()
    own_rows.wait()


def return_rows(part, gate_part, n_ep, n_tp):
    _, cap, features = part.shape
    width = features // n_tp
    chunks = n_ep if n_ep <= 8 else next(c for c in range(8, 0, -1) if n_ep % c == 0)
    n_y = n_tp // 2
    dma = pltpu.SemaphoreType.DMA
    return pl.pallas_call(
        functools.partial(return_kernel, n_ep, n_tp, chunks),
        out_shape=(
            jax.ShapeDtypeStruct((n_ep, cap, width), BF16),
            jax.ShapeDtypeStruct(gate_part.shape, F32),
        ),
        in_specs=[pl.BlockSpec(memory_space=pltpu.VMEM)] * 2,
        out_specs=[pl.BlockSpec(memory_space=pltpu.VMEM)] * 2,
        scratch_shapes=[
            pltpu.VMEM((n_y, n_ep, cap, width), BF16),
            pltpu.VMEM((n_y, n_ep, cap, width), BF16),
            pltpu.VMEM((n_y, n_ep, cap, width), BF16),
            pltpu.VMEM((n_ep, cap, width), BF16),
            pltpu.VMEM((n_tp,) + gate_part.shape, F32),
            pltpu.VMEM(gate_part.shape, F32),
            dma((n_y, chunks)),
            dma((n_y, chunks)),
            dma((n_y, chunks)),
            dma((n_y, chunks)),
            dma((n_ep,)),
            dma((n_ep,)),
            dma((n_tp,)),
            dma((n_tp,)),
            dma((n_ep,)),
            dma((n_ep,)),
            dma((2,)),
        ],
        compiler_params=pltpu.CompilerParams(collective_id=1, has_side_effects=True),
        name="return_rows",
    )(part, gate_part)


def sums_kernel(
    n_ep,
    n_tp,
    square_ref,
    term_ref,
    square_out,
    term_out,
    square_buf,
    term_buf,
    tp_send,
    tp_recv,
    ep_send,
    ep_recv,
):
    ep, tp, _, _ = place()
    greet(n_ep, n_tp, True)

    def tp_copy(dst, src):
        return pltpu.make_async_remote_copy(
            src_ref=square_ref,
            dst_ref=square_buf.at[src],
            send_sem=tp_send.at[dst],
            recv_sem=tp_recv.at[src],
            device_id=(ep, dst),
            device_id_type=MESH,
        )

    def ep_copy(dst, src):
        return pltpu.make_async_remote_copy(
            src_ref=term_ref.at[dst],
            dst_ref=term_buf.at[src],
            send_sem=ep_send.at[dst],
            recv_sem=ep_recv.at[src],
            device_id=(dst, tp),
            device_id_type=MESH,
        )

    loop(1, n_ep, lambda r: ep_copy(lax.rem(ep + r, n_ep), ep).start())
    loop(1, n_tp, lambda r: tp_copy(lax.rem(tp + r, n_tp), tp).start())
    square = square_ref[...]
    for r in range(1, n_tp):
        source = lax.rem(tp + r, n_tp)
        tp_copy(tp, source).wait_recv()
        square = square + square_buf[source]
    square_out[...] = square
    term_out[...] = term_ref[ep]

    def add(r):
        source = lax.rem(ep + r, n_ep)
        ep_copy(ep, source).wait_recv()
        term_out[...] += term_buf[source]

    loop(1, n_ep, add)
    loop(1, n_ep, lambda r: ep_copy(lax.rem(ep + r, n_ep), ep).wait_send())
    loop(1, n_tp, lambda r: tp_copy(lax.rem(tp + r, n_tp), tp).wait_send())


def small_sums(square, term, n_ep, n_tp):
    dma = pltpu.SemaphoreType.DMA
    return pl.pallas_call(
        functools.partial(sums_kernel, n_ep, n_tp),
        out_shape=(
            jax.ShapeDtypeStruct(square.shape, F32),
            jax.ShapeDtypeStruct(term.shape[1:], F32),
        ),
        in_specs=[pl.BlockSpec(memory_space=pltpu.VMEM)] * 2,
        out_specs=[pl.BlockSpec(memory_space=pltpu.VMEM)] * 2,
        scratch_shapes=[
            pltpu.VMEM((n_tp,) + square.shape, F32),
            pltpu.VMEM(term.shape, F32),
            dma((n_tp,)),
            dma((n_tp,)),
            dma((n_ep,)),
            dma((n_ep,)),
        ],
        compiler_params=pltpu.CompilerParams(collective_id=2, has_side_effects=True),
        name="small_sums",
    )(square, term)


def weight_grads_kernel(x_ref, gate_ref, up_ref, gate_out, up_out, square_out):
    rows = x_ref.shape[1]
    for row, (grad, out) in enumerate(((gate_ref, gate_out), (up_ref, up_out))):
        total = matmul_tn(x_ref[...], grad[...])
        out[0] = total.astype(BF16)
        square = jnp.sum(total * total, axis=1, keepdims=True)
        square_out[row : row + 1, :] = jnp.broadcast_to(square, (rows, 128)).T[0:1, :]


def weight_grads(full_input, gate_pre_grad, up_pre_grad):
    slots, features = full_input.shape
    hidden = gate_pre_grad.shape[1]
    rows = min(512, features)
    whole = pl.BlockSpec((slots, hidden), lambda i: (0, 0))
    grad = pl.BlockSpec((1, rows, hidden), lambda i: (0, i, 0))
    return pl.pallas_call(
        weight_grads_kernel,
        grid=(features // rows,),
        out_shape=(
            jax.ShapeDtypeStruct((1, features, hidden), BF16),
            jax.ShapeDtypeStruct((1, features, hidden), BF16),
            jax.ShapeDtypeStruct((2, features), F32),
        ),
        in_specs=[pl.BlockSpec((slots, rows), lambda i: (0, i)), whole, whole],
        out_specs=[grad, grad, pl.BlockSpec((2, rows), lambda i: (0, i))],
        cost_estimate=pl.CostEstimate(
            flops=4 * slots * features * hidden,
            bytes_accessed=4 * features * hidden + 2 * slots * features,
            transcendentals=0,
        ),
        name="weight_grads",
    )(full_input, gate_pre_grad, up_pre_grad)


def combine_kernel(
    table_ref,
    back_ref,
    back_gate_ref,
    routes_ref,
    weights_ref,
    tokens_ref,
    router_ref,
    token_out,
    gate_out,
    term_out,
):
    n_ep, cap, width = back_ref.shape
    top, tok = routes_ref.shape
    padded = back_gate_ref.shape[2]
    tp = lax.axis_index("tp")
    table = table_ref[...]
    routes = routes_ref[...]
    weights = weights_ref[...].astype(F32)
    labels = lax.broadcasted_iota(jnp.int32, (n_ep, tok), 0)
    exact = dict(precision=lax.Precision.HIGHEST, preferred_element_type=F32)
    slot_gate = back_gate_ref[:, 0, :]
    spread = lax.dot_general(
        slot_gate, lane_pick(n_ep, cap, padded), (((1,), (1,)), ((), ())), **exact
    )
    values = jnp.dot(spread * own_block(n_ep, cap), table.astype(F32), **exact)
    grads = []
    mixed = jnp.zeros((1, tok), F32)
    for k in range(top):
        same = routes[k : k + 1, :] == labels
        grads.append(jnp.sum(jnp.where(same, values, 0.0), axis=0, keepdims=True))
        gate_out[k : k + 1, :] = grads[k]
        mixed = mixed + weights[k : k + 1, :] * grads[k]
    signal = jnp.zeros((n_ep, tok), F32)
    for k in range(top):
        logit = weights[k : k + 1, :] * (grads[k] - mixed)
        signal = signal + jnp.where(routes[k : k + 1, :] == labels, logit, 0.0)
    signal = signal.astype(BF16)
    term = jnp.dot(signal, tokens_ref[...], preferred_element_type=F32)
    for e in range(n_ep):
        term_out[e] = term[e : e + 1, :]
    back = back_ref[...].astype(F32).reshape(n_ep * cap, width).astype(BF16)
    cols = pl.ds(pl.multiple_of(tp * width, width), width)
    token_out[...] = matmul_tn(table, back) + matmul_tn(signal, router_ref[:, cols])


def combine(table, back_rows, back_gate, routes, weights, tokens, router_rows):
    experts = router_rows.shape[0]
    return pl.pallas_call(
        combine_kernel,
        out_shape=(
            jax.ShapeDtypeStruct(tokens.shape, F32),
            jax.ShapeDtypeStruct(routes.shape, F32),
            jax.ShapeDtypeStruct((experts, 1, tokens.shape[1]), F32),
        ),
        in_specs=[pl.BlockSpec(memory_space=pltpu.VMEM)] * 7,
        out_specs=[pl.BlockSpec(memory_space=pltpu.VMEM)] * 3,
        name="combine",
    )(table, back_rows, back_gate, routes, weights, tokens, router_rows)


def lanes(slot_values, experts, capacity):
    padded = -(-capacity // 128) * 128
    rows = jnp.pad(slot_values.reshape(experts, 1, capacity), ((0, 0), (0, 7), (0, padded - capacity)))
    return rows


def shards(tokens, routing, gate_weights, cotangent, expert_gate, expert_up, expert_down, router):
    tok_rows, local_width = tokens.shape
    top_count = routing.shape[1]
    experts = router.shape[1]
    n_tp = lax.axis_size("tp")
    n_ep = lax.axis_size("ep")
    capacity = 3 * top_count * tok_rows // (2 * experts)
    slot_count = experts * capacity
    features = local_width * n_tp
    routes, weights = routing.T, gate_weights.T
    full_input, full_tangent, weight_slots, table = dispatch(
        routes, weights, tokens, cotangent, n_ep, n_tp, capacity
    )
    full_input = full_input.reshape(slot_count, features)
    full_tangent = full_tangent.reshape(slot_count, features)
    slot_weight = weight_slots[:, 0, :capacity].reshape(slot_count, 1)
    gate_matrix = expert_gate[0]
    up_matrix = expert_up[0]
    down_matrix = expert_down[0]
    hidden_local = gate_matrix.shape[1]
    pre_gate = jnp.dot(full_input, gate_matrix, preferred_element_type=F32)
    pre_up = jnp.dot(full_input, up_matrix, preferred_element_type=F32)
    back_proj = matmul_nt(full_tangent, down_matrix)
    sigmoid_gate = jax.nn.sigmoid(pre_gate)
    active = pre_gate * sigmoid_gate
    hidden = active * pre_up
    slot_part = jnp.sum(hidden * back_proj, axis=1)
    scaled = (slot_weight * hidden).astype(BF16)
    hidden_grad = slot_weight * back_proj
    gate_pre_grad = (
        hidden_grad * pre_up * sigmoid_gate * (1.0 + pre_gate * (1.0 - sigmoid_gate))
    ).astype(BF16)
    up_pre_grad = (hidden_grad * active).astype(BF16)
    gate_proj_grad, up_proj_grad, squares = weight_grads(full_input, gate_pre_grad, up_pre_grad)
    down_sum = matmul_tn(scaled, full_tangent)
    unit_count = hidden_local * n_tp
    slot_grad = (
        matmul_nt(gate_pre_grad, gate_matrix) + matmul_nt(up_pre_grad, up_matrix)
    ).astype(BF16)
    back_rows, back_gate = return_rows(
        slot_grad.reshape(experts, capacity, features),
        lanes(slot_part, experts, capacity),
        n_ep,
        n_tp,
    )
    token_grad, gate_grad, router_term = combine(
        table, back_rows, back_gate, routes, weights, tokens, router.T
    )
    squares, router_grad = small_sums(squares, router_term, n_ep, n_tp)
    return (
        token_grad,
        gate_grad.T,
        gate_proj_grad,
        up_proj_grad,
        down_sum.astype(BF16)[None],
        router_grad,
        squares[0:1] / unit_count,
        squares[1:2] / unit_count,
        jnp.mean(down_sum * down_sum, axis=1)[None, :],
    )


def solution(mesh):
    in_specs = (
        P("ep", "tp"),
        P("ep", None),
        P("ep", None),
        P("ep", "tp"),
        P("ep", None, "tp"),
        P("ep", None, "tp"),
        P("ep", "tp", None),
        P(),
    )
    out_specs = (
        P("ep", "tp"),
        P("ep", None),
        P("ep", None, "tp"),
        P("ep", None, "tp"),
        P("ep", "tp", None),
        P("ep", "tp"),
        P("ep", None),
        P("ep", None),
        P("ep", "tp"),
    )
    return jax.shard_map(shards, mesh=mesh, in_specs=in_specs, out_specs=out_specs, check_vma=False)
```

profile of v0, /device:TPU:0, one launch (start us, length us, event | category | flops | bytes accessed | tf_op | source)
XLA Modules:
  0.0 100.0 jit_solution(15567720080325406733)
XLA Ops:
  0.6 0.0 copy-start
  0.7 35.4 %dispatch.1 = (bf16[8,48,2048]{2,1,0:T(8,128)(2,1)}, bf16[8,48,2048]{2,1,0:T(8,128)(2,1)}, f32[8,8,128]{2,1,0:T(8,128)}, bf16[384,128]{1,0:T(8,128)(2,1)}) custom-call(s32[2,128]{1,0:T(2,128)} %bitcast.34, bf16[2,128]{1,0:T(2,128)(2,1)} %bitcast.36, bf16[128,512]{1,0:T(8,128)(2,1)} %tokens_ref.3, bf16[128,512]{1,0:T(8,128)(2,1)} %cotangent_ref.1), custom_call_target="tpu_custom_call" | custom-call | tf_op jit(solution)/shard_map/dispatch/pallas_call | solution.py:280
  36.1 0.8 slice_reduce_fusion
  36.9 0.1 mul.43
  37.0 0.0 copy-done
  37.0 0.0 copy-start.2
  37.0 0.0 copy-start.4
  37.0 2.9 %fusion.2 = f32[384,768]{1,0:T(8,128)S(1)} fusion(bf16[384,2048]{1,0:T(8,128)(2,1)} %bitcast.38, bf16[1,2048,768]{2,1,0:T(8,128)(2,1)S(1)} %copy-done), kind=kOutput, calls=%fused_computation.3 | convolution fusion | flops 1207959552 | bytes 5898240 | tf_op jit(solution)/shard_map/dot_general | solution.py:712
  39.9 0.0 copy-done.2
  39.9 0.0 copy-done.4
  39.9 0.0 copy-start.1
  39.9 0.0 copy-start.5
  40.0 1.4 %fusion.6 = f32[384,768]{1,0:T(8,128)S(1)} fusion(bf16[384,2048]{1,0:T(8,128)(2,1)S(1)} %bitcast.40, bf16[1,2048,768]{2,1,0:T(8,128)(2,1)S(1)} %copy-done.2), kind=kOutput, calls=%fused_computation.7 | convolution fusion | flops 1207959552 | bytes 5898240 | tf_op jit(solution)/shard_map/dot_general | solution.py:713
  41.4 0.5 copy-done.1
  41.8 0.5 copy-done.5
  42.3 2.9 %multiply_reduce_fusion.1 = (f32[384]{0:T(512)S(1)}, bf16[384,768]{1,0:T(8,128)(2,1)}, bf16[384,768]{1,0:T(8,128)(2,1)}) fusion(f32[384,768]{1,0:T(8,128)S(1)} %fusion.6, f32[384,768]{1,0:T(8,128)S(1)} %fusion.2, f32[384]{0:T(512)S(1)} %mul.43, bf16[384,2048]{1,0:T(8,128)(2,1)S(1)} %bitcast.41, bf16[1,768,2048]{2,1,0:T(8,128)(2,1)S(1)} %copy-done.1), kind=kOutput, calls=%fused_computation.14 | convolution fusion | flops 1212972672 | bytes 8260608 | tf_op jit(solution)/shard_map/dot_general | solution.py:22
  45.2 3.6 %multiply_reduce_fusion = (f32[768]{0:T(1024)S(1)}, bf16[1,768,2048]{2,1,0:T(8,128)(2,1)}) fusion(bf16[384,2048]{1,0:T(8,128)(2,1)S(1)} %bitcast.42, f32[384]{0:T(512)S(1)} %mul.43, f32[384,768]{1,0:T(8,128)S(1)} %fusion.6, f32[384,768]{1,0:T(8,128)S(1)} %fusion.2), kind=kOutput, calls=%fused_computation | convolution fusion | flops 1214741760 | bytes 7082496 | tf_op jit(solution)/shard_map/dot_general | solution.py:16
  48.8 0.6 div.22
  49.4 0.1 reshape.43
  49.5 0.6 pad.4.gate_ref
  50.1 0.0 copy-start.3
  50.1 0.0 copy-start.6
  50.1 2.6 %fusion = f32[384,2048]{1,0:T(8,128)S(1)} fusion(bf16[384,768]{1,0:T(8,128)(2,1)} %get-tuple-element.40.gate_ref, bf16[1,2048,768]{2,1,0:T(8,128)(2,1)S(1)} %copy-done), kind=kOutput, calls=%fused_computation.1 | convolution fusion | flops 1207959552 | bytes 6881280 | tf_op jit(solution)/shard_map/dot_general | solution.py:22
  52.7 0.0 copy-done.3
  52.7 0.0 copy-done.6
  52.8 2.6 %add_convert_fusion = bf16[384,2048]{1,0:T(8,128)(2,1)} fusion(f32[384,2048]{1,0:T(8,128)S(1)} %fusion, bf16[384,768]{1,0:T(8,128)(2,1)S(1)} %copy-done.6, bf16[1,2048,768]{2,1,0:T(8,128)(2,1)S(1)} %copy-done.3), kind=kOutput, calls=%fused_computation.12 | convolution fusion | flops 1209532416 | bytes 8454144 | tf_op jit(solution)/shard_map/dot_general | solution.py:22
  55.3 23.4 %return_rows.1 = (bf16[8,48,512]{2,1,0:T(8,128)(2,1)}, f32[8,8,128]{2,1,0:T(8,128)}) custom-call(bf16[8,48,2048]{2,1,0:T(8,128)(2,1)} %bitcast.32, f32[8,8,128]{2,1,0:T(8,128)} %pad.4.gate_ref), custom_call_target="tpu_custom_call" | custom-call | tf_op jit(solution)/shard_map/return_rows/pallas_call | solution.py:479
  78.8 2.8 %combine.1 = (f32[128,512]{1,0:T(8,128)}, f32[2,128]{1,0:T(2,128)}, f32[8,1,512]{2,1,0:T(1,128)}) custom-call(bf16[384,128]{1,0:T(8,128)(2,1)} %get-tuple-element.23.table_ref, bf16[8,48,512]{2,1,0:T(8,128)(2,1)} %get-tuple-element.27.back_ref, f32[8,8,128]{2,1,0:T(8,128)} %get-tuple-element.28.back_gate_ref, s32[2,128]{1,0:T(2,128)} %bitcast.35, ...), custom_call_target="tpu_custom_call" | custom-call | tf_op jit(solution)/shard_map/combine/pallas_call | solution.py:673
  81.5 6.9 %weight_grads.1 = (bf16[1,2048,768]{2,1,0:T(8,128)(2,1)}, bf16[1,2048,768]{2,1,0:T(8,128)(2,1)}, f32[2,2048]{1,0:T(2,128)}) custom-call(bf16[384,2048]{1,0:T(8,128)(2,1)} %bitcast.39, bf16[384,768]{1,0:T(8,128)(2,1)} %get-tuple-element.40.gate_ref, bf16[384,768]{1,0:T(8,128)(2,1)} %get-tuple-element.41.up_ref), custom_call_target="tpu_custom_call" | custom-call | flops 2415919104 | bytes 7864320 | tf_op jit(solution)/shard_map/weight_grads/pallas_call | solution.py:606
  88.4 8.8 %small_sums.1 = (f32[2,2048]{1,0:T(2,128)}, f32[1,512]{1,0:T(1,128)}) custom-call(f32[2,2048]{1,0:T(2,128)} %get-tuple-element.33.square_ref, f32[8,1,512]{2,1,0:T(1,128)} %get-tuple-element.34.term_ref), custom_call_target="tpu_custom_call" | custom-call | tf_op jit(solution)/shard_map/small_sums/pallas_call | solution.py:570
  97.3 1.4 %slice_multiply_fusion = (f32[1,2048]{1,0:T(1,128)}, f32[1,2048]{1,0:T(1,128)}) fusion(f32[2,2048]{1,0:T(2,128)} %get-tuple-element.36), kind=kLoop, calls=%fused_computation.22 | loop fusion | flops 4096 | bytes 32768 | tf_op jit(solution)/shard_map/div | solution.py:749
  98.7 1.3 %copy.18 = f32[1,512]{1,0:T(1,128)} copy(f32[1,512]{1,0:T(1,128)} %get-tuple-element.58) | data formatting | bytes 4096
  (1 shorter events, 0.0 us)
Async XLA Ops:
  0.6 36.3 %copy-start = (bf16[1,2048,768]{2,1,0:T(8,128)(2,1)S(1)}, bf16[1,2048,768]{2,1,0:T(8,128)(2,1)}, u32[]{:S(2)}) copy-start(bf16[1,2048,768]{2,1,0:T(8,128)(2,1)} %param.12) | copy-start | bytes 9437188
  37.0 3.0 %copy-start.2 = (bf16[1,2048,768]{2,1,0:T(8,128)(2,1)S(1)}, bf16[1,2048,768]{2,1,0:T(8,128)(2,1)}, u32[]{:S(2)}) copy-start(bf16[1,2048,768]{2,1,0:T(8,128)(2,1)} %param.13) | copy-start | bytes 9437188
  37.0 3.0 %copy-start.4 = (bf16[8,48,2048]{2,1,0:T(8,128)(2,1)S(1)}, bf16[8,48,2048]{2,1,0:T(8,128)(2,1)}, u32[]{:S(2)}) copy-start(bf16[8,48,2048]{2,1,0:T(8,128)(2,1)} %get-tuple-element.26) | copy-start | bytes 4718596
  39.9 1.9 %copy-start.1 = (bf16[1,768,2048]{2,1,0:T(8,128)(2,1)S(1)}, bf16[1,768,2048]{2,1,0:T(8,128)(2,1)}, u32[]{:S(2)}) copy-start(bf16[1,768,2048]{2,1,0:T(8,128)(2,1)} %param.14) | copy-start | bytes 9437188
  39.9 2.3 %copy-start.5 = (bf16[8,48,2048]{2,1,0:T(8,128)(2,1)S(1)}, bf16[8,48,2048]{2,1,0:T(8,128)(2,1)}, u32[]{:S(2)}) copy-start(bf16[8,48,2048]{2,1,0:T(8,128)(2,1)} %get-tuple-element.25) | copy-start | bytes 4718596
  50.1 2.6 %copy-start.3 = (bf16[1,2048,768]{2,1,0:T(8,128)(2,1)S(1)}, bf16[1,2048,768]{2,1,0:T(8,128)(2,1)}, u32[]{:S(2)}) copy-start(bf16[1,2048,768]{2,1,0:T(8,128)(2,1)} %param.13) | copy-start | bytes 9437188
  50.1 2.6 %copy-start.6 = (bf16[384,768]{1,0:T(8,128)(2,1)S(1)}, bf16[384,768]{1,0:T(8,128)(2,1)}, u32[]{:S(2)}) copy-start(bf16[384,768]{1,0:T(8,128)(2,1)} %get-tuple-element.41.up_ref) | copy-start | bytes 1769476
where the time goes:
time: 101 us; the launch traced here: 100 us
  Pallas kernels  77.4 us (77%)
  matrix products  16 us (16%)
  local copies, waits for them, and re-layouts  4.38 us (4%)
  other arithmetic  1.42 us (1%)
    pallas_call x1, Pallas kernels, dispatch(): pl.pallas_call(functools.partial(dispatch_kernel, n_ep, n_tp, chunks), ou...  35.4 us
    pallas_call x1, Pallas kernels, return_rows(): pl.pallas_call(functools.partial(return_kernel, n_ep, n_tp, chunks), out_...  23.4 us
    pallas_call x1, Pallas kernels, small_sums(): pl.pallas_call(functools.partial(sums_kernel, n_ep, n_tp), out_shape=(jax...  8.83 us
    dot_general x3, matrix products, matmul_nt(): lax.dot_general(left_side, right_side, (((1,), (1,)), ((), ())), preferre...  8.06 us
    pallas_call x1, Pallas kernels, weight_grads(): pl.pallas_call(weight_grads_kernel, grid=(features // rows,), out_shape=(...  6.9 us
    dot_general x1, matrix products, matmul_tn(): lax.dot_general(left_side, right_side, (((0,), (0,)), ((), ())), preferre...  3.64 us
    dot_general x1, matrix products, shards(): pre_gate = jnp.dot(full_input, gate_matrix, preferred_element_type=F32)  2.93 us
    pallas_call x1, Pallas kernels, combine(): pl.pallas_call(combine_kernel, out_shape=(jax.ShapeDtypeStruct(tokens.sha...  2.78 us

commit v1 on v0

v1 whole, which is shorter than its diff:
```python
import functools

import jax
import jax.numpy as jnp
from jax import lax
from jax.experimental import pallas as pl
from jax.experimental.pallas import tpu as pltpu
from jax.sharding import PartitionSpec as P

MESH = pl.DeviceIdType.MESH
F32 = jnp.float32
BF16 = jnp.bfloat16
VMEM = pltpu.VMEM


def matmul_nn(left_side, right_side):
    return jnp.dot(left_side, right_side, preferred_element_type=F32)


def matmul_tn(left_side, right_side):
    return lax.dot_general(
        left_side, right_side, (((0,), (0,)), ((), ())), preferred_element_type=F32
    )


def matmul_nt(left_side, right_side):
    return lax.dot_general(
        left_side, right_side, (((1,), (1,)), ((), ())), preferred_element_type=F32
    )


def loop(lower, upper, body):
    if upper - lower <= 8:
        for i in range(lower, upper):
            body(i)
    else:
        lax.fori_loop(lower, upper, lambda i, carry: (body(i), carry)[1], 0)


def place():
    ep, tp = lax.axis_index("ep"), lax.axis_index("tp")
    return ep, tp, lax.div(tp, 2), lax.rem(tp, 2)


def paired(value, step, count):
    if count & (count - 1):
        return lax.rem(value + step, count)
    out, bit = value, 1
    while bit < count:
        asked = lax.rem(lax.div(jnp.int32(step), bit), 2)
        out = out + asked * bit * (1 - 2 * lax.rem(lax.div(value, bit), 2))
        bit *= 2
    return out


def greet(n_ep, n_tp, between=None):
    ep, tp, _, _ = place()
    barrier = pltpu.get_barrier_semaphore()

    def to_ep(r):
        pl.semaphore_signal(
            barrier, inc=1, device_id=(lax.rem(ep + r, n_ep), tp), device_id_type=MESH
        )

    def to_tp(r):
        pl.semaphore_signal(
            barrier, inc=1, device_id=(ep, lax.rem(tp + r, n_tp)), device_id_type=MESH
        )

    loop(1, n_ep, to_ep)
    loop(1, n_tp, to_tp)
    if between is not None:
        between()
    pl.semaphore_wait(barrier, n_ep - 1 + n_tp - 1)


def lane_pick(n_ep, cap):
    shape = (n_ep, cap, 128)
    pick = lax.broadcasted_iota(jnp.int32, shape, 1) == lax.broadcasted_iota(jnp.int32, shape, 2)
    return pick.astype(F32).reshape(n_ep * cap, 128)


def own_block(n_ep, cap):
    shape = (n_ep, n_ep * cap)
    first = lax.broadcasted_iota(jnp.int32, shape, 0) * cap
    slot = lax.broadcasted_iota(jnp.int32, shape, 1)
    return ((slot >= first) & (slot < first + cap)).astype(F32)


def fill_slots(cap, routes_ref, weights_ref, tokens_ref, cotangent_ref, table_ref, out_ref, w_ref):
    n_ep = w_ref.shape[0]
    width = out_ref.shape[2]
    top, tok = routes_ref.shape
    routes = routes_ref[...]
    weights = weights_ref[...].astype(F32)
    labels = lax.broadcasted_iota(jnp.int32, (n_ep, tok), 0)
    hit = jnp.zeros((n_ep, tok), F32)
    chosen = jnp.zeros((n_ep, tok), F32)
    for k in range(top):
        same = routes[k : k + 1, :] == labels
        hit = hit + same.astype(F32)
        chosen = chosen + jnp.where(same, weights[k : k + 1, :], 0.0)
    square = (tok, tok)
    before = lax.broadcasted_iota(jnp.int32, square, 0) < lax.broadcasted_iota(jnp.int32, square, 1)
    count = matmul_nn(hit.astype(BF16), before.astype(F32).astype(BF16))
    position = jnp.where(hit > 0.0, count, -1.0)
    slot = lax.broadcasted_iota(jnp.int32, (n_ep, cap, tok), 1).astype(F32)
    table = (slot == position[:, None, :]).astype(F32).reshape(n_ep * cap, tok).astype(BF16)
    table_ref[...] = table
    for which, source in enumerate((tokens_ref, cotangent_ref)):
        out_ref[which] = matmul_nn(table, source[...]).astype(BF16)
    spread = matmul_nt(chosen.astype(BF16), table) * own_block(n_ep, cap)
    values = matmul_nn(spread.astype(BF16), lane_pick(n_ep, cap).astype(BF16))
    w_ref[...] = jnp.broadcast_to(values[:, None, :], w_ref.shape)


def layer_kernel(
    n_ep,
    n_tp,
    chunks,
    cap,
    routes_ref,
    weights_ref,
    tokens_ref,
    cotangent_ref,
    router_ref,
    gate_hbm,
    up_hbm,
    down_hbm,
    token_out,
    gate_out,
    term_out,
    square_out,
    down_square_out,
    gate_res,
    up_res,
    down_res,
    gate_w,
    up_w,
    down_w,
    table_ref,
    slots_ref,
    w_ref,
    full_ref,
    full_w_ref,
    pre_gate,
    pre_up,
    back_proj,
    slot_w,
    slot_sum,
    scaled_ref,
    gate_pre,
    up_pre,
    part_ref,
    gate_send_ref,
    gate_buf,
    gate_back_out,
    gate_back,
    core_buf,
    y_out,
    y_buf,
    ep_out,
    back_ref,
    square_buf,
    term_ref,
    term_buf,
    load_sem,
    own_sem,
    ep_send,
    ep_recv,
    w_send,
    w_recv,
    y_send,
    y_recv,
    core_send,
    core_recv,
    rcore_send,
    rcore_recv,
    ry_send,
    ry_recv,
    rep_send,
    rep_recv,
    tp_send,
    tp_recv,
    gate_sem_send,
    gate_sem_recv,
    sq_send,
    sq_recv,
    term_send,
    term_recv,
):
    ep, tp, y, core = place()
    n_y = n_tp // 2
    partner = y * 2 + 1 - core
    slots, features = part_ref.shape
    width = features // n_tp
    hidden = gate_w.shape[1]
    top, tok = routes_ref.shape
    per = n_ep // chunks
    rows = per * cap
    size = 2 if chunks % 2 == 0 else 1
    groups = chunks // size
    group_rows = size * rows
    exact_rows = 16 if group_rows % 16 == 0 else 8

    def cols(which):
        return pl.ds(pl.multiple_of(which * width, width), width)

    def chunk_rows(chunk):
        return pl.ds(pl.multiple_of(chunk * rows, rows), rows)

    def source_rows(source):
        return pl.ds(pl.multiple_of(source * cap, cap), cap)

    def remote(src, dst, send, recv, device):
        return pltpu.make_async_remote_copy(
            src_ref=src,
            dst_ref=dst,
            send_sem=send,
            recv_sem=recv,
            device_id=device,
            device_id_type=MESH,
        )

    def group_at(j):
        return paired(lax.div(ep, per * size), j, groups)

    def chunk_at(j, i):
        return group_at(j) * size + (i if size == 1 else lax.rem(lax.div(ep, per) + i, size))

    def ep_copy(dst, src):
        return remote(
            slots_ref.at[:, source_rows(dst), :],
            full_ref.at[:, source_rows(src), cols(tp)],
            ep_send.at[dst],
            ep_recv.at[src],
            (dst, tp),
        )

    def w_copy(dst, src):
        return remote(w_ref.at[dst], full_w_ref.at[src], w_send.at[dst], w_recv.at[src], (dst, tp))

    def y_copy(source_y, target_y, chunk):
        piece = full_ref.at[:, chunk_rows(chunk), cols(source_y * 2 + core)]
        return remote(
            piece,
            piece,
            y_send.at[target_y, chunk],
            y_recv.at[source_y, chunk],
            (ep, target_y * 2 + core),
        )

    def core_copy(source_y, source_core, chunk):
        piece = full_ref.at[:, chunk_rows(chunk), cols(source_y * 2 + source_core)]
        return remote(
            piece, piece, core_send.at[source_y, chunk], core_recv.at[source_y, chunk], (ep, partner)
        )

    def rcore_copy(target_y, chunk):
        return remote(
            part_ref.at[chunk_rows(chunk), cols(target_y * 2 + 1 - core)],
            core_buf.at[target_y, chunk_rows(chunk)],
            rcore_send.at[target_y, chunk],
            rcore_recv.at[target_y, chunk],
            (ep, partner),
        )

    def ry_copy(source_y, target_y, chunk):
        return remote(
            y_out.at[target_y, chunk_rows(chunk)],
            y_buf.at[source_y, chunk_rows(chunk)],
            ry_send.at[target_y, chunk],
            ry_recv.at[source_y, chunk],
            (ep, target_y * 2 + core),
        )

    def rep_copy(dst, src):
        return remote(
            ep_out.at[source_rows(dst)],
            back_ref.at[source_rows(src)],
            rep_send.at[dst],
            rep_recv.at[src],
            (dst, tp),
        )

    def tp_copy(dst, src):
        return remote(gate_send_ref, gate_buf.at[src], tp_send.at[dst], tp_recv.at[src], (ep, dst))

    def gate_copy(dst, src):
        return remote(
            gate_back_out.at[dst],
            gate_back.at[src],
            gate_sem_send.at[dst],
            gate_sem_recv.at[src],
            (dst, tp),
        )

    def square_copy(dst, src):
        return remote(
            square_buf.at[src], square_buf.at[src], sq_send.at[dst], sq_recv.at[src], (ep, dst)
        )

    def term_copy(dst, src):
        return remote(
            term_ref.at[dst], term_buf.at[src], term_send.at[dst], term_recv.at[src], (dst, tp)
        )

    loads = [
        pltpu.make_async_copy(hbm.at[0], vmem, load_sem.at[i])
        for i, (hbm, vmem) in enumerate(((gate_hbm, gate_w), (up_hbm, up_w), (down_hbm, down_w)))
    ]
    for load in loads:
        load.start()
    fill = functools.partial(
        fill_slots,
        cap,
        routes_ref,
        weights_ref,
        tokens_ref,
        cotangent_ref,
        table_ref,
        slots_ref,
        w_ref,
    )
    greet(n_ep, n_tp, fill)

    own_rows = pltpu.make_async_copy(
        slots_ref.at[:, source_rows(ep), :],
        full_ref.at[:, source_rows(ep), cols(tp)],
        own_sem.at[0],
    )
    own_w = pltpu.make_async_copy(w_ref.at[ep], full_w_ref.at[ep], own_sem.at[1])
    own_rows.start()
    own_w.start()

    def each_source(j, i, body):
        chunk = chunk_at(j, i)

        def one(n):
            source = chunk * per + n

            @pl.when(source != ep)
            def _():
                body(source)

        loop(0, per, one)

    def send_group(j):
        for i in range(size):
            each_source(j, i, lambda dst: ep_copy(dst, ep).start())

    loop(0, groups, send_group)

    def send_w_group(j):
        for i in range(size):
            each_source(j, i, lambda dst: w_copy(dst, ep).start())

    loop(0, groups, send_w_group)
    gate_send_ref[...] = jnp.zeros_like(gate_send_ref)
    own_rows.wait()
    own_w.wait()

    def relay(j):
        for i in range(size):
            chunk = chunk_at(j, i)
            each_source(j, i, lambda source: ep_copy(ep, source).wait_recv())
            for r in range(1, n_y):
                y_copy(y, lax.rem(y + r, n_y), chunk).start()
            core_copy(y, core, chunk).start()

    def forward(j):
        for i in range(size):
            chunk = chunk_at(j, i)
            for r in range(1, n_y):
                source_y = lax.rem(y + n_y - r, n_y)
                y_copy(source_y, y, chunk).wait_recv()
                core_copy(source_y, core, chunk).start()

    def arrive(j):
        for i in range(size):
            chunk = chunk_at(j, i)
            for r in range(n_y):
                core_copy(r, 1 - core, chunk).wait_recv()
            each_source(j, i, lambda source: w_copy(ep, source).wait_recv())

    def compute(j):
        group = group_at(j)
        at = pl.ds(pl.multiple_of(group * group_rows, group_rows), group_rows)
        first = group * (size * per)
        for n in range(size * per):
            weight = jnp.broadcast_to(full_w_ref[first + n][0:1, :], (128, 128)).T
            slot_w[n * cap : (n + 1) * cap, :] = weight[0:cap, :]
        x = full_ref[0, at, :]
        pre_gate[...] = matmul_nn(x, gate_w[...])
        pre_up[...] = matmul_nn(x, up_w[...])
        back_proj[...] = matmul_nt(full_ref[1, at, :], down_w[...])
        part_cols = 256 if hidden % 256 == 0 else hidden

        def block(b):
            here = pl.ds(pl.multiple_of(b * exact_rows, exact_rows), exact_rows)
            there = pl.ds(
                pl.multiple_of(group * group_rows + b * exact_rows, exact_rows), exact_rows
            )
            weight = slot_w[here, 0:1]
            total = jnp.zeros((exact_rows, 1), F32)
            for c in range(0, hidden, part_cols):
                span = slice(c, c + part_cols)
                gate = pre_gate[here, span]
                up = pre_up[here, span]
                back = back_proj[here, span]
                sigmoid = jax.nn.sigmoid(gate)
                active = gate * sigmoid
                value = active * up
                total = total + jnp.sum(value * back, axis=1, keepdims=True)
                scaled_ref[there, span] = (weight * value).astype(BF16)
                grad = weight * back
                gate_pre[there, span] = (
                    grad * up * sigmoid * (1.0 + gate * (1.0 - sigmoid))
                ).astype(BF16)
                up_pre[there, span] = (grad * active).astype(BF16)
            slot_sum[here, :] = jnp.broadcast_to(total, (exact_rows, 128))

        lax.fori_loop(0, group_rows // exact_rows, lambda b, c: (block(b), c)[1], 0)
        gate_rows = gate_pre[at, :]
        up_rows = up_pre[at, :]
        part_ref[at, :] = (matmul_nt(gate_rows, gate_w[...]) + matmul_nt(up_rows, up_w[...])).astype(
            BF16
        )
        for n in range(size * per):
            column = slot_sum[n * cap : (n + 1) * cap, :]
            block_sum = jnp.concatenate([column, jnp.zeros((128 - cap, 128), F32)], axis=0)
            gate_send_ref[first + n] = jnp.broadcast_to(block_sum.T[0:1, :], (8, 128))

    def send_part(j):
        for i in range(size):
            chunk = chunk_at(j, i)
            for r in range(n_y):
                rcore_copy(lax.rem(y + r + 1, n_y), chunk).start()

    def across(j):
        for i in range(size):
            chunk = chunk_at(j, i)
            here = chunk_rows(chunk)
            for r in range(1, n_y):
                target = lax.rem(y + r, n_y)
                rcore_copy(target, chunk).wait_recv()
                mine = part_ref[here, cols(target * 2 + core)].astype(F32)
                y_out[target, here] = (mine + core_buf[target, here].astype(F32)).astype(BF16)
                ry_copy(y, target, chunk).start()

    def scatter(j):
        for i in range(size):
            chunk = chunk_at(j, i)
            here = chunk_rows(chunk)
            rcore_copy(y, chunk).wait_recv()
            value = part_ref[here, cols(tp)].astype(F32) + core_buf[y, here].astype(F32)
            for r in range(1, n_y):
                source = lax.rem(y + r, n_y)
                ry_copy(source, y, chunk).wait_recv()
                value = value + y_buf[source, here].astype(F32)
            ep_out[here, :] = value.astype(BF16)
            each_source(j, i, lambda dst: rep_copy(dst, ep).start())

    for load in loads:
        load.wait()

    def step(s, carry):
        @pl.when(s < groups)
        def _():
            relay(s)

        @pl.when(s >= 1)
        def _():
            forward(s - 1)
            arrive(s - 1)
            compute(s - 1)
            send_part(s - 1)

        @pl.when(s >= 2)
        def _():
            across(s - 2)

        @pl.when(s >= 3)
        def _():
            scatter(s - 3)

        return carry

    lax.fori_loop(0, groups + 1, step, 0)

    loop(1, n_tp, lambda r: tp_copy(lax.rem(tp + r, n_tp), tp).start())
    gate_buf[tp] = gate_send_ref[...]

    tile = 256 if features % 256 == 0 else features
    tiles = features // tile

    def gate_tile(i, carry):
        span = pl.ds(pl.multiple_of(i * tile, tile), tile)
        x = full_ref[0, :, span]
        for row, (grad, out) in enumerate(((gate_pre, gate_res), (up_pre, up_res))):
            total = matmul_tn(x, grad[...])
            out[0, span, :] = total.astype(BF16)
            square = jnp.sum(total * total, axis=1, keepdims=True)
            square_buf[tp, row : row + 1, span] = jnp.broadcast_to(square, (tile, 128)).T[0:1, :]
        return carry

    down_tile = 256 if hidden % 256 == 0 else hidden
    tangents = full_ref.at[1]

    def down_part(i):
        span = slice(i * down_tile, (i + 1) * down_tile)
        total = matmul_tn(scaled_ref[:, span], tangents[...])
        down_res[0, span, :] = total.astype(BF16)
        square = jnp.sum(total * total, axis=1, keepdims=True)
        down_square_out[0:1, span] = jnp.broadcast_to(square, (down_tile, 128)).T[0:1, :] / features

    split = tiles // 2
    across(groups - 1)
    for i in range(hidden // down_tile):
        down_part(i)
    total = jnp.zeros(gate_send_ref.shape, F32)
    for r in range(1, n_tp):
        tp_copy(tp, lax.rem(tp + r, n_tp)).wait_recv()
    for r in range(n_tp):
        total = total + gate_buf[r]
    gate_back_out[...] = total
    loop(1, n_ep, lambda r: gate_copy(lax.rem(ep + r, n_ep), ep).start())
    gate_back[ep] = gate_back_out[ep]
    for j in range(max(groups - 2, 0), groups):
        scatter(j)
    own_back = pltpu.make_async_copy(
        ep_out.at[source_rows(ep)], back_ref.at[source_rows(ep)], own_sem.at[2]
    )
    own_back.start()
    lax.fori_loop(0, split, gate_tile, 0)

    loop(1, n_ep, lambda r: gate_copy(ep, lax.rem(ep + r, n_ep)).wait_recv())
    routes = routes_ref[...]
    weights = weights_ref[...].astype(F32)
    labels = lax.broadcasted_iota(jnp.int32, (n_ep, tok), 0)
    rest = gate_back[:, 0, :]
    pieces = []
    for _ in range(3):
        pieces.append(rest.astype(BF16).astype(F32))
        rest = rest - pieces[-1]
    picked = matmul_nt(
        jnp.concatenate(pieces, axis=0).astype(BF16), lane_pick(n_ep, cap).astype(BF16)
    )
    mask = own_block(n_ep, cap)
    spread = (picked * jnp.concatenate([mask] * 3, axis=0)).astype(BF16)
    parts = matmul_nn(spread, table_ref[...])
    values = (parts[0:n_ep] + parts[n_ep : 2 * n_ep]) + parts[2 * n_ep :]
    grads = []
    mixed = jnp.zeros((1, tok), F32)
    for k in range(top):
        same = routes[k : k + 1, :] == labels
        grads.append(jnp.sum(jnp.where(same, values, 0.0), axis=0, keepdims=True))
        gate_out[k : k + 1, :] = grads[k]
        mixed = mixed + weights[k : k + 1, :] * grads[k]
    signal = jnp.zeros((n_ep, tok), F32)
    for k in range(top):
        logit = weights[k : k + 1, :] * (grads[k] - mixed)
        signal = signal + jnp.where(routes[k : k + 1, :] == labels, logit, 0.0)
    signal = signal.astype(BF16)
    term = matmul_nn(signal, tokens_ref[...])
    for e in range(n_ep):
        term_ref[e] = term[e : e + 1, :]
    loop(1, n_ep, lambda r: term_copy(lax.rem(ep + r, n_ep), ep).start())
    term_buf[ep] = term_ref[ep]
    lax.fori_loop(split, tiles, gate_tile, 0)
    loop(1, n_tp, lambda r: square_copy(lax.rem(tp + r, n_tp), tp).start())

    own_back.wait()
    loop(1, n_ep, lambda r: rep_copy(ep, lax.rem(ep + r, n_ep)).wait_recv())
    token_out[...] = matmul_tn(table_ref[...], back_ref[...]) + matmul_tn(
        signal, router_ref[:, cols(tp)]
    )
    loop(1, n_ep, lambda r: term_copy(ep, lax.rem(ep + r, n_ep)).wait_recv())
    term_total = term_buf[0]
    for e in range(1, n_ep):
        term_total = term_total + term_buf[e]
    term_out[...] = term_total
    for r in range(1, n_tp):
        square_copy(tp, lax.rem(tp + r, n_tp)).wait_recv()
    square = square_buf[0]
    for r in range(1, n_tp):
        square = square + square_buf[r]
    square_out[...] = square / (hidden * n_tp)

    def drain_ep(r):
        other = lax.rem(ep + r, n_ep)
        for copy in (ep_copy, w_copy, rep_copy, gate_copy, term_copy):
            copy(other, ep).wait_send()

    loop(1, n_ep, drain_ep)

    def drain_tp(r):
        other = lax.rem(tp + r, n_tp)
        tp_copy(other, tp).wait_send()
        square_copy(other, tp).wait_send()

    loop(1, n_tp, drain_tp)

    def drain_chunk(chunk):
        for r in range(n_y):
            core_copy(r, core, chunk).wait_send()
            rcore_copy(r, chunk).wait_send()
        for r in range(1, n_y):
            y_copy(y, lax.rem(y + r, n_y), chunk).wait_send()
            ry_copy(y, lax.rem(y + r, n_y), chunk).wait_send()

    loop(0, chunks, drain_chunk)


def layer(routes, weights, tokens, cotangent, router_rows, gate, up, down, n_ep, n_tp, cap):
    tok, width = tokens.shape
    features, hidden = gate.shape[1:]
    chunks = n_ep if n_ep <= 8 else next(c for c in range(8, 0, -1) if n_ep % c == 0)
    size = 2 if chunks % 2 == 0 else 1
    n_y = n_tp // 2
    slots = n_ep * cap
    group_rows = slots // chunks * size
    dma = pltpu.SemaphoreType.DMA
    in_vmem = pl.BlockSpec(memory_space=VMEM)
    in_hbm = pl.BlockSpec(memory_space=pltpu.HBM)
    return pl.pallas_call(
        functools.partial(layer_kernel, n_ep, n_tp, chunks, cap),
        out_shape=(
            VMEM((tok, width), F32),
            VMEM(routes.shape, F32),
            VMEM((1, width), F32),
            VMEM((2, features), F32),
            VMEM((1, hidden), F32),
            VMEM(gate.shape, BF16),
            VMEM(up.shape, BF16),
            VMEM(down.shape, BF16),
        ),
        in_specs=[in_vmem] * 5 + [in_hbm] * 3,
        out_specs=[in_vmem] * 8,
        scratch_shapes=[
            VMEM((features, hidden), BF16),
            VMEM((features, hidden), BF16),
            VMEM((hidden, features), BF16),
            VMEM((slots, tok), BF16),
            VMEM((2, slots, width), BF16),
            VMEM((n_ep, 8, 128), F32),
            VMEM((2, slots, features), BF16),
            VMEM((n_ep, 8, 128), F32),
            VMEM((group_rows, hidden), F32),
            VMEM((group_rows, hidden), F32),
            VMEM((group_rows, hidden), F32),
            VMEM((group_rows, 128), F32),
            VMEM((group_rows, 128), F32),
            VMEM((slots, hidden), BF16),
            VMEM((slots, hidden), BF16),
            VMEM((slots, hidden), BF16),
            VMEM((slots, features), BF16),
            VMEM((n_ep, 8, 128), F32),
            VMEM((n_tp, n_ep, 8, 128), F32),
            VMEM((n_ep, 8, 128), F32),
            VMEM((n_ep, 8, 128), F32),
            VMEM((n_y, slots, width), BF16),
            VMEM((n_y, slots, width), BF16),
            VMEM((n_y, slots, width), BF16),
            VMEM((slots, width), BF16),
            VMEM((slots, width), BF16),
            VMEM((n_tp, 2, features), F32),
            VMEM((n_ep, 1, width), F32),
            VMEM((n_ep, 1, width), F32),
            dma((3,)),
            dma((3,)),
            dma((n_ep,)),
            dma((n_ep,)),
            dma((n_ep,)),
            dma((n_ep,)),
            dma((n_y, chunks)),
            dma((n_y, chunks)),
            dma((n_y, chunks)),
            dma((n_y, chunks)),
            dma((n_y, chunks)),
            dma((n_y, chunks)),
            dma((n_y, chunks)),
            dma((n_y, chunks)),
            dma((n_ep,)),
            dma((n_ep,)),
            dma((n_tp,)),
            dma((n_tp,)),
            dma((n_ep,)),
            dma((n_ep,)),
            dma((n_tp,)),
            dma((n_tp,)),
            dma((n_ep,)),
            dma((n_ep,)),
        ],
        compiler_params=pltpu.CompilerParams(
            collective_id=0, has_side_effects=True, vmem_limit_bytes=48 * 2**20
        ),
        name="layer",
    )(routes, weights, tokens, cotangent, router_rows, gate, up, down)


def write_kernel(count, *refs):
    ins, outs, sems = refs[:count], refs[count : 2 * count], refs[-1]
    copies = [
        pltpu.make_async_copy(source, target, sems.at[i])
        for i, (source, target) in enumerate(zip(ins, outs, strict=True))
    ]
    for copy in copies:
        copy.start()
    for copy in copies:
        copy.wait()


def write_out(*arrays):
    count = len(arrays)
    return pl.pallas_call(
        functools.partial(write_kernel, count),
        out_shape=tuple(jax.ShapeDtypeStruct(a.shape, a.dtype) for a in arrays),
        in_specs=[pl.BlockSpec(memory_space=VMEM)] * count,
        out_specs=[pl.BlockSpec(memory_space=pltpu.HBM)] * count,
        scratch_shapes=[pltpu.SemaphoreType.DMA((count,))],
        compiler_params=pltpu.CompilerParams(vmem_limit_bytes=2**20),
        name="write_out",
    )(*(pltpu.with_memory_space_constraint(a, VMEM) for a in arrays))


def shards(tokens, routing, gate_weights, cotangent, expert_gate, expert_up, expert_down, router):
    tok_rows = tokens.shape[0]
    top_count = routing.shape[1]
    experts = router.shape[1]
    n_tp = lax.axis_size("tp")
    n_ep = lax.axis_size("ep")
    capacity = 3 * top_count * tok_rows // (2 * experts)
    results = layer(
        routing.T,
        gate_weights.T,
        tokens,
        cotangent,
        router.T,
        expert_gate,
        expert_up,
        expert_down,
        n_ep,
        n_tp,
        capacity,
    )
    token_grad, gate_grad, router_grad, squares, down_squares, gates, ups, downs = write_out(*results)
    return (
        token_grad,
        gate_grad.T,
        gates,
        ups,
        downs,
        router_grad,
        squares[0:1],
        squares[1:2],
        down_squares,
    )


def solution(mesh):
    in_specs = (
        P("ep", "tp"),
        P("ep", None),
        P("ep", None),
        P("ep", "tp"),
        P("ep", None, "tp"),
        P("ep", None, "tp"),
        P("ep", "tp", None),
        P(),
    )
    out_specs = (
        P("ep", "tp"),
        P("ep", None),
        P("ep", None, "tp"),
        P("ep", None, "tp"),
        P("ep", "tp", None),
        P("ep", "tp"),
        P("ep", None),
        P("ep", None),
        P("ep", "tp"),
    )
    return jax.shard_map(shards, mesh=mesh, in_specs=in_specs, out_specs=out_specs, check_vma=False)
```

time: 101 us -> 69.8 us (0.69)
  matrix products: 16 us -> 0 us
  Pallas kernels: 77.4 us -> 68.4 us
  local copies, waits for them, and re-layouts: 4.38 us -> 0.62 us
  other arithmetic: 1.42 us -> 0 us
    dot_general x6 -> x0, matrix products: 16 us -> none  [the longest x3 8.06 us: matmul_nt(): lax.dot_general(left_side, right_side, (((1,), (1,)), ((), ())), preferre...]
    pallas_call x5 -> x2, Pallas kernels: 77.4 us -> 68.4 us  [the longest x1 64.5 us: layer(): pl.pallas_call(functools.partial(layer_kernel, n_ep, n_tp, chunks, cap),...]
    unnamed x15 -> x0, local copies, waits for them, and re-layouts: 2.23 us -> none
    div x2 -> x0, other arithmetic: 1.42 us -> none  [the longest x1 1.41 us: shards(): squares[1:2] / unit_count]
where the time goes in v1:
time: 69.8 us; the launch traced here: 69.6 us
  Pallas kernels  68.4 us (98%)
    pallas_call x1, Pallas kernels, layer(): pl.pallas_call(functools.partial(layer_kernel, n_ep, n_tp, chunks, cap),...  64.5 us
    pallas_call x1, Pallas kernels, write_out(): pl.pallas_call(functools.partial(write_kernel, count), out_shape=tuple((j...  3.91 us

profile of v1, /device:TPU:0, one launch (start us, length us, event | category | flops | bytes accessed | tf_op | source)
XLA Modules:
  0.0 69.6 jit_solution(15844269382799500139)
XLA Ops:
  0.6 64.5 %layer.1 = (f32[128,512]{1,0:T(8,128)S(1)}, f32[2,128]{1,0:T(2,128)S(1)}, f32[1,512]{1,0:T(1,128)S(1)}, f32[2,2048]{1,0:T(2,128)S(1)}, f32[1,768]{1,0:T(1,128)S(...) custom-call(s32[2,128]{1,0:T(2,128)} %bitcast.5, ...), custom_call_target="tpu_custom_call" | custom-call | tf_op jit(solution)/shard_map/layer/pallas_call | solution.py:626
  65.1 3.9 %write_out.1 = (f32[128,512]{1,0:T(8,128)}, f32[2,128]{1,0:T(2,128)}, f32[1,512]{1,0:T(1,128)}, f32[2,2048]{1,0:T(2,128)S(1)}, f32[1,768]{1,0:T(1,128)}, /*index...) custom-call(f32[128,512]{1,0:T(8,128)S(1)} %get-tuple-element.25.refs_0_, ...), custom_call_target="tpu_custom_call" | custom-call | tf_op jit(solution)/shard_map/write_out/pallas_call | solution.py:716
  69.0 0.6 fusion

commit v2 on v1

v2 whole, which is shorter than its diff:
```python
import functools

import jax
import jax.numpy as jnp
from jax import lax
from jax.experimental import pallas as pl
from jax.experimental.pallas import tpu as pltpu
from jax.sharding import PartitionSpec as P

MESH = pl.DeviceIdType.MESH
F32 = jnp.float32
BF16 = jnp.bfloat16
VMEM = pltpu.VMEM


def matmul_nn(left_side, right_side):
    return jnp.dot(left_side, right_side, preferred_element_type=F32)


def matmul_tn(left_side, right_side):
    return lax.dot_general(
        left_side, right_side, (((0,), (0,)), ((), ())), preferred_element_type=F32
    )


def matmul_nt(left_side, right_side):
    return lax.dot_general(
        left_side, right_side, (((1,), (1,)), ((), ())), preferred_element_type=F32
    )


def loop(lower, upper, body):
    if upper - lower <= 8:
        for i in range(lower, upper):
            body(i)
    else:
        lax.fori_loop(lower, upper, lambda i, carry: (body(i), carry)[1], 0)


def place():
    ep, tp = lax.axis_index("ep"), lax.axis_index("tp")
    return ep, tp, lax.div(tp, 2), lax.rem(tp, 2)


def paired(value, step, count):
    if count & (count - 1):
        return lax.rem(value + step, count)
    out, bit = value, 1
    while bit < count:
        asked = lax.rem(lax.div(jnp.int32(step), bit), 2)
        out = out + asked * bit * (1 - 2 * lax.rem(lax.div(value, bit), 2))
        bit *= 2
    return out


def greet(n_ep, n_tp, between=None):
    ep, tp, _, _ = place()
    barrier = pltpu.get_barrier_semaphore()

    def to_ep(r):
        pl.semaphore_signal(
            barrier, inc=1, device_id=(lax.rem(ep + r, n_ep), tp), device_id_type=MESH
        )

    def to_tp(r):
        pl.semaphore_signal(
            barrier, inc=1, device_id=(ep, lax.rem(tp + r, n_tp)), device_id_type=MESH
        )

    loop(1, n_ep, to_ep)
    loop(1, n_tp, to_tp)
    if between is not None:
        between()
    pl.semaphore_wait(barrier, n_ep - 1 + n_tp - 1)


def lane_pick(n_ep, cap):
    shape = (n_ep, cap, 128)
    pick = lax.broadcasted_iota(jnp.int32, shape, 1) == lax.broadcasted_iota(jnp.int32, shape, 2)
    return pick.astype(F32).reshape(n_ep * cap, 128)


def own_block(n_ep, cap):
    shape = (n_ep, n_ep * cap)
    first = lax.broadcasted_iota(jnp.int32, shape, 0) * cap
    slot = lax.broadcasted_iota(jnp.int32, shape, 1)
    return ((slot >= first) & (slot < first + cap)).astype(F32)


def fill_slots(cap, routes_ref, weights_ref, tokens_ref, cotangent_ref, table_ref, out_ref, w_ref):
    n_ep = w_ref.shape[0]
    width = out_ref.shape[2]
    top, tok = routes_ref.shape
    routes = routes_ref[...]
    weights = weights_ref[...].astype(F32)
    labels = lax.broadcasted_iota(jnp.int32, (n_ep, tok), 0)
    hit = jnp.zeros((n_ep, tok), F32)
    chosen = jnp.zeros((n_ep, tok), F32)
    for k in range(top):
        same = routes[k : k + 1, :] == labels
        hit = hit + same.astype(F32)
        chosen = chosen + jnp.where(same, weights[k : k + 1, :], 0.0)
    square = (tok, tok)
    before = lax.broadcasted_iota(jnp.int32, square, 0) < lax.broadcasted_iota(jnp.int32, square, 1)
    count = matmul_nn(hit.astype(BF16), before.astype(F32).astype(BF16))
    position = jnp.where(hit > 0.0, count, -1.0)
    slot = lax.broadcasted_iota(jnp.int32, (n_ep, cap, tok), 1).astype(F32)
    table = (slot == position[:, None, :]).astype(F32).reshape(n_ep * cap, tok).astype(BF16)
    table_ref[...] = table
    for which, source in enumerate((tokens_ref, cotangent_ref)):
        out_ref[which] = matmul_nn(table, source[...]).astype(BF16)
    spread = matmul_nt(chosen.astype(BF16), table) * own_block(n_ep, cap)
    values = matmul_nn(spread.astype(BF16), lane_pick(n_ep, cap).astype(BF16))
    w_ref[...] = jnp.broadcast_to(values[:, None, :], w_ref.shape)


def layer_kernel(
    n_ep,
    n_tp,
    chunks,
    cap,
    routes_hbm,
    weights_hbm,
    tokens_hbm,
    cotangent_hbm,
    router_hbm,
    gate_hbm,
    up_hbm,
    down_hbm,
    token_out,
    gate_out,
    term_out,
    gate_square_out,
    up_square_out,
    down_square_out,
    gate_res,
    up_res,
    down_res,
    routes_ref,
    weights_ref,
    tokens_ref,
    cotangent_ref,
    router_ref,
    gate_w,
    up_w,
    down_w,
    gate_t,
    up_t,
    down_t,
    table_ref,
    slots_ref,
    w_ref,
    full_ref,
    full_w_ref,
    pre_gate,
    pre_up,
    back_proj,
    slot_w,
    slot_sum,
    scaled_ref,
    gate_pre,
    up_pre,
    part_ref,
    gate_send_ref,
    gate_buf,
    gate_back_out,
    gate_back,
    core_buf,
    y_out,
    y_buf,
    ep_out,
    back_ref,
    square_buf,
    term_ref,
    term_buf,
    load_sem,
    own_sem,
    send_sem,
    all_recv,
    ep_recv,
    y_recv,
    core_recv,
    rcore_recv,
    ry_recv,
):
    ep, tp, y, core = place()
    n_y = n_tp // 2
    partner = y * 2 + 1 - core
    slots, features = part_ref.shape
    width = features // n_tp
    hidden = gate_w.shape[1]
    top, tok = routes_ref.shape
    per = n_ep // chunks
    rows = per * cap
    size = 2 if chunks % 2 == 0 else 1
    groups = chunks // size
    group_rows = size * rows
    exact_rows = 16 if group_rows % 16 == 0 else 8

    batches, backs = batches_of(groups)

    def cols(which):
        return pl.ds(pl.multiple_of(which * width, width), width)

    def y_cols(which):
        return pl.ds(pl.multiple_of(which * (2 * width), 2 * width), 2 * width)

    def base_of(j, count):
        return lax.div(group_at(j), count) * count

    def group_range(j, count, start=0, many=None):
        first = base_of(j, count) * group_rows + start
        return pl.ds(
            pl.multiple_of(first, exact_rows), count * group_rows if many is None else many
        )

    def batch_rows(batch, start=0, many=None):
        return group_range(*batches[batch], start, many)

    def chunk_rows(chunk):
        return pl.ds(pl.multiple_of(chunk * rows, rows), rows)

    def source_rows(source):
        return pl.ds(pl.multiple_of(source * cap, cap), cap)

    def remote(src, dst, send, recv, device):
        return pltpu.make_async_remote_copy(
            src_ref=src,
            dst_ref=dst,
            send_sem=send,
            recv_sem=recv,
            device_id=device,
            device_id_type=MESH,
        )

    def group_at(j):
        return paired(lax.div(ep, per * size), j, groups)

    def chunk_at(j, i):
        return group_at(j) * size + paired(lax.rem(lax.div(ep, per), size), i, size)

    def ep_copy(dst, src):
        return remote(
            slots_ref.at[:, source_rows(dst), :],
            full_ref.at[:, source_rows(src), cols(tp)],
            send_sem.at[0],
            ep_recv.at[src],
            (dst, tp),
        )

    def w_copy(dst, src):
        return remote(w_ref.at[dst], full_w_ref.at[src], send_sem.at[1], all_recv.at[0], (dst, tp))

    def y_copy(source_y, target_y, chunk, r):
        piece = full_ref.at[:, chunk_rows(chunk), cols(source_y * 2 + core)]
        return remote(
            piece, piece, send_sem.at[2], y_recv.at[r - 1, chunk], (ep, target_y * 2 + core)
        )

    def core_copy(source_y, source_core, at, slot, batch):
        piece = full_ref.at[:, at, cols(source_y * 2 + source_core)]
        return remote(piece, piece, send_sem.at[3], core_recv.at[slot, batch], (ep, partner))

    def rcore_copy(target_y, j, count, slot, back):
        at = group_range(j, count)
        return remote(
            part_ref.at[at, cols(target_y * 2 + 1 - core)],
            core_buf.at[target_y, at],
            send_sem.at[4],
            rcore_recv.at[slot, back],
            (ep, partner),
        )

    def ry_copy(source_y, target_y, chunk, r):
        return remote(
            y_out.at[target_y, chunk_rows(chunk)],
            y_buf.at[source_y, chunk_rows(chunk)],
            send_sem.at[5],
            ry_recv.at[r - 1, chunk],
            (ep, target_y * 2 + core),
        )

    def rep_copy(dst, src):
        return remote(
            ep_out.at[source_rows(dst)],
            back_ref.at[source_rows(src)],
            send_sem.at[6],
            all_recv.at[1],
            (dst, tp),
        )

    def tp_copy(dst, src):
        return remote(
            gate_send_ref, gate_buf.at[src], send_sem.at[7], all_recv.at[2], (ep, dst)
        )

    def gate_copy(dst, src):
        return remote(
            gate_back_out.at[dst], gate_back.at[src], send_sem.at[8], all_recv.at[3], (dst, tp)
        )

    def square_copy(dst, src):
        return remote(
            square_buf.at[src], square_buf.at[src], send_sem.at[9], all_recv.at[4], (ep, dst)
        )

    def term_copy(dst, src):
        return remote(
            term_ref.at[dst], term_buf.at[src], send_sem.at[10], all_recv.at[5], (dst, tp)
        )

    def whole(ref, send=None, recv=None):
        copy = remote(
            ref,
            ref,
            send_sem.at[0 if send is None else send],
            all_recv.at[0 if recv is None else recv],
            (ep, partner),
        )
        if send is not None:
            copy.wait_send()
        if recv is not None:
            copy.wait_recv()

    others = n_ep - 1

    pairs = (
        (routes_hbm, routes_ref),
        (weights_hbm, weights_ref),
        (tokens_hbm, tokens_ref),
        (cotangent_hbm, cotangent_ref),
        (gate_hbm.at[0], gate_w),
        (up_hbm.at[0], up_w),
        (down_hbm.at[0], down_w),
        (router_hbm, router_ref),
    )
    loads = [pltpu.make_async_copy(*pair, load_sem.at[i]) for i, pair in enumerate(pairs)]

    def begin():
        for load in loads:
            load.start()
        for load in loads[:4]:
            load.wait()
        fill()

    fill = functools.partial(
        fill_slots,
        cap,
        routes_ref,
        weights_ref,
        tokens_ref,
        cotangent_ref,
        table_ref,
        slots_ref,
        w_ref,
    )
    greet(n_ep, n_tp, begin)

    own_rows = pltpu.make_async_copy(
        slots_ref.at[:, source_rows(ep), :],
        full_ref.at[:, source_rows(ep), cols(tp)],
        own_sem.at[0],
    )
    own_w = pltpu.make_async_copy(w_ref.at[ep], full_w_ref.at[ep], own_sem.at[1])
    own_rows.start()
    own_w.start()

    def each_source(j, i, body):
        chunk = chunk_at(j, i)

        def one(n):
            source = chunk * per + n

            @pl.when(source != ep)
            def _():
                body(source)

        loop(0, per, one)

    def send_group(j):
        for i in range(size):
            each_source(j, i, lambda dst: ep_copy(dst, ep).start())

    loop(1, n_ep, lambda r: w_copy(lax.rem(ep + r, n_ep), ep).start())
    loop(0, groups, send_group)
    gate_send_ref[...] = jnp.zeros_like(gate_send_ref)
    own_rows.wait()
    own_w.wait()

    def batch_of(j):
        return next(b for b, (k, count) in enumerate(batches) if k <= j < k + count)

    def relay(j, i):
        chunk = chunk_at(j, i)
        each_source(j, i, lambda source: ep_copy(ep, source).wait_recv())
        for r in range(1, n_y):
            y_copy(y, lax.rem(y + r, n_y), chunk, r).start()
        core_copy(y, core, chunk_rows(chunk), 0, batch_of(j)).start()

    def forward(j, i):
        chunk = chunk_at(j, i)
        for r in range(1, n_y):
            source_y = lax.rem(y + n_y - r, n_y)
            y_copy(source_y, y, chunk, r).wait_recv()
            core_copy(source_y, core, chunk_rows(chunk), r, batch_of(j)).start()

    def chunks_of(batch):
        j, count = batches[batch]
        return [(k, i) for k in range(j, j + count) for i in range(size)]

    def back_chunks(back):
        j, count = backs[back]
        return [(k, i) for k in range(j, j + count) for i in range(size)]

    def multiply(batch, which, first):
        at = batch_rows(batch)
        many = batches[batch][1] * group_rows
        k = y_cols(which)
        x, t = full_ref[0, at, k], full_ref[1, at, k]
        for out, value in (
            (pre_gate, matmul_nn(x, gate_w[k, :])),
            (pre_up, matmul_nn(x, up_w[k, :])),
            (back_proj, matmul_nn(t, down_t[k, :])),
        ):
            out[0:many, :] = value if first else out[0:many, :] + value

    def near_product(batch):
        core_copy(y, 1 - core, batch_rows(batch), 0, batch).wait_recv()
        multiply(batch, y, True)

    def far_product(batch):
        for r in range(1, n_y):
            source_y = lax.rem(y + n_y - r, n_y)
            core_copy(source_y, 1 - core, batch_rows(batch), r, batch).wait_recv()
            multiply(batch, source_y, False)

    part_cols = 256 if hidden % 256 == 0 else hidden
    lane_sums = part_cols % 128 == 0
    first_lane = lax.broadcasted_iota(jnp.int32, (exact_rows, 128), 1) == 0

    def gradients(batch):
        first = base_of(*batches[batch]) * (size * per)
        many = batches[batch][1] * size * per
        for n in range(many):
            weight = jnp.broadcast_to(full_w_ref[first + n][0:1, :], (128, 128)).T
            slot_w[n * cap : (n + 1) * cap, :] = weight[0:cap, :]
        for b in range(0, many * cap, exact_rows):
            here = slice(b, b + exact_rows)
            there = batch_rows(batch, b, exact_rows)
            weight = slot_w[here, 0:1]
            total = jnp.zeros((exact_rows, 128), F32)
            for c in range(0, hidden, part_cols):
                span = slice(c, c + part_cols)
                gate = pre_gate[here, span]
                up = pre_up[here, span]
                back = back_proj[here, span]
                sigmoid = 0.5 * jnp.tanh(0.5 * gate) + 0.5
                active = gate * sigmoid
                value = active * up
                product = value * back
                if lane_sums:
                    for lane in range(0, part_cols, 128):
                        total = total + product[:, lane : lane + 128]
                else:
                    row = jnp.sum(product, axis=1, keepdims=True)
                    total = total + jnp.where(first_lane, row, 0.0)
                scaled_ref[there, span] = (weight * value).astype(BF16)
                grad = weight * back
                gate_pre[there, span] = (
                    grad * up * (sigmoid * (1.0 + gate * (1.0 - sigmoid)))
                ).astype(BF16)
                up_pre[there, span] = (grad * active).astype(BF16)
            slot_sum[here, :] = jnp.broadcast_to(
                jnp.sum(total, axis=1, keepdims=True), (exact_rows, 128)
            )
        for n in range(many):
            column = slot_sum[n * cap : (n + 1) * cap, :]
            block_sum = jnp.concatenate([column, jnp.zeros((128 - cap, 128), F32)], axis=0)
            gate_send_ref[first + n] = jnp.broadcast_to(block_sum.T[0:1, :], (8, 128))

    def slot_grads(back, r, own):
        j, count = backs[back]
        at = group_range(j, count)
        target = lax.rem(y + r, n_y)
        block = cols(target * 2 + (core if own else 1 - core))
        part_ref[at, block] = (
            matmul_nn(gate_pre[at, :], gate_t[:, block]) + matmul_nn(up_pre[at, :], up_t[:, block])
        ).astype(BF16)
        if not own:
            rcore_copy(target, j, count, r, back).start()

    def across(back):
        for r in range(1, n_y):
            target = lax.rem(y + r, n_y)
            rcore_copy(target, *backs[back], r, back).wait_recv()
            for j, i in back_chunks(back):
                chunk = chunk_at(j, i)
                here = chunk_rows(chunk)
                mine = part_ref[here, cols(target * 2 + core)].astype(F32)
                y_out[target, here] = (mine + core_buf[target, here].astype(F32)).astype(BF16)
                ry_copy(y, target, chunk, r).start()

    def own_arrives(back):
        rcore_copy(y, *backs[back], 0, back).wait_recv()

    def scatter(j, i):
        chunk = chunk_at(j, i)
        here = chunk_rows(chunk)
        value = part_ref[here, cols(tp)].astype(F32) + core_buf[y, here].astype(F32)
        for r in range(1, n_y):
            source = lax.rem(y + n_y - r, n_y)
            ry_copy(source, y, chunk, r).wait_recv()
            value = value + y_buf[source, here].astype(F32)
        ep_out[here, :] = value.astype(BF16)
        each_source(j, i, lambda dst: rep_copy(dst, ep).start())

    for load in loads[4:]:
        load.wait()

    def each(chosen, body):
        for j, i in chosen:
            body(j, i)

    def slots_other(back):
        for r in range(1, n_y):
            slot_grads(back, r, False)
            slot_grads(back, r, True)

    def slots_own(back):
        slot_grads(back, 0, False)
        across(back)
        slot_grads(back, 0, True)

    def prep_tile(source, target, turns):
        def turn(i, carry):
            span = pl.ds(pl.multiple_of(i * 256, 256), 256)
            target[:, span] = source[span, :].T
            return carry

        lax.fori_loop(0, turns, turn, 0)

    def prep_down():
        span = 256 if hidden % 256 == 0 else hidden
        for c in range(0, hidden, span):
            down_t[:, c : c + span] = down_w[c : c + span, :].T

    prep_down()
    last = len(batches) - 1
    ready = {k + count - 1: b for b, (k, count) in enumerate(backs)}
    each(chunks_of(0)[:2], relay)
    prep_tile(gate_w, gate_t, features // 256)
    each(chunks_of(0)[2:], relay)
    prep_tile(up_w, up_t, features // 256)
    near_product(0)
    whole(full_w_ref.at[pl.ds(0, others)], recv=0)
    pending = None
    for b in range(last):
        later = chunks_of(b + 1)
        if b == 0:
            each(later[:1], relay)
            each(chunks_of(0), forward)
            each(later[1:], relay)
        far_product(b)
        gradients(b)
        near_product(b + 1)
        after = chunks_of(b + 2) if b + 2 <= last else []
        each(after[:1], relay)
        each(later, forward)
        if pending is not None:
            slots_own(pending)
            pending = None
        done = ready.get(sum(batches[b]) - 1)
        if done is not None:
            slots_other(done)
            pending = done
        each(after[1:], relay)
    if pending is not None:
        slots_own(pending)
    if last == 0:
        each(chunks_of(0), forward)
    far_product(last)
    gradients(last)
    loop(1, n_tp, lambda r: tp_copy(lax.rem(tp + r, n_tp), tp).start())
    gate_buf[tp] = gate_send_ref[...]
    final = len(backs) - 1
    slots_other(final)

    def add_gates():
        whole(gate_buf.at[pl.ds(0, n_tp - 1)], recv=2)
        total = gate_buf[0]
        for r in range(1, n_tp):
            total = total + gate_buf[r]
        gate_back_out[...] = total
        loop(1, n_ep, lambda r: gate_copy(lax.rem(ep + r, n_ep), ep).start())
        gate_back[ep] = gate_back_out[ep]

    slots_own(final)

    tile = 256 if features % 256 == 0 else features
    tiles = features // tile

    def gate_tile(i, carry):
        span = pl.ds(pl.multiple_of(i * tile, tile), tile)
        x = full_ref[0, :, span]
        for row, (grad, out) in enumerate(((gate_pre, gate_res), (up_pre, up_res))):
            total = matmul_tn(x, grad[...])
            out[0, span, :] = total.astype(BF16)
            square = jnp.sum(total * total, axis=1, keepdims=True)
            square_buf[tp, row : row + 1, span] = jnp.broadcast_to(square, (tile, 128)).T[0:1, :]
        return carry

    down_tile = 256 if hidden % 256 == 0 else hidden
    tangents = full_ref.at[1]

    def down_part(i):
        span = slice(i * down_tile, (i + 1) * down_tile)
        total = matmul_tn(scaled_ref[:, span], tangents[...])
        down_res[0, span, :] = total.astype(BF16)
        square = jnp.sum(total * total, axis=1, keepdims=True)
        down_square_out[0:1, span] = jnp.broadcast_to(square, (down_tile, 128)).T[0:1, :] / features

    early = min(2, tiles)
    middle = min(tiles, early + 2)
    chosen = back_chunks(final)
    half = (len(chosen) + 1) // 2
    for b in range(final):
        own_arrives(b)
        each(back_chunks(b), scatter)
    lax.fori_loop(0, 1, gate_tile, 0)
    add_gates()
    lax.fori_loop(1, early, gate_tile, 0)
    own_arrives(final)
    each(chosen[:half], scatter)
    lax.fori_loop(early, middle, gate_tile, 0)

    whole(gate_back.at[pl.ds(0, others)], recv=3)
    routes = routes_ref[...]
    weights = weights_ref[...].astype(F32)
    labels = lax.broadcasted_iota(jnp.int32, (n_ep, tok), 0)
    rest = gate_back[:, 0, :]
    pieces = []
    for _ in range(3):
        pieces.append(rest.astype(BF16).astype(F32))
        rest = rest - pieces[-1]
    picked = matmul_nt(
        jnp.concatenate(pieces, axis=0).astype(BF16), lane_pick(n_ep, cap).astype(BF16)
    )
    mask = own_block(n_ep, cap)
    spread = (picked * jnp.concatenate([mask] * 3, axis=0)).astype(BF16)
    parts = matmul_nn(spread, table_ref[...])
    values = (parts[0:n_ep] + parts[n_ep : 2 * n_ep]) + parts[2 * n_ep :]
    grads = []
    mixed = jnp.zeros((1, tok), F32)
    for k in range(top):
        same = routes[k : k + 1, :] == labels
        grads.append(jnp.sum(jnp.where(same, values, 0.0), axis=0, keepdims=True))
        gate_out[k : k + 1, :] = grads[k]
        mixed = mixed + weights[k : k + 1, :] * grads[k]
    signal = jnp.zeros((n_ep, tok), F32)
    for k in range(top):
        logit = weights[k : k + 1, :] * (grads[k] - mixed)
        signal = signal + jnp.where(routes[k : k + 1, :] == labels, logit, 0.0)
    signal = signal.astype(BF16)
    term = matmul_nn(signal, tokens_ref[...])
    for e in range(n_ep):
        term_ref[e] = term[e : e + 1, :]
    loop(1, n_ep, lambda r: term_copy(lax.rem(ep + r, n_ep), ep).start())
    term_buf[ep] = term_ref[ep]
    each(chosen[half:], scatter)
    own_back = pltpu.make_async_copy(
        ep_out.at[source_rows(ep)], back_ref.at[source_rows(ep)], own_sem.at[2]
    )
    own_back.start()
    lax.fori_loop(middle, tiles, gate_tile, 0)
    loop(1, n_tp, lambda r: square_copy(lax.rem(tp + r, n_tp), tp).start())
    for i in range(hidden // down_tile):
        down_part(i)
    part_slots = pl.ds(0, others * cap)
    whole(slots_ref.at[:, part_slots], send=0)
    whole(full_w_ref.at[pl.ds(0, others)], send=1)
    whole(full_ref.at[:, :, pl.ds(0, (n_y - 1) * width)], send=2)
    whole(full_ref.at[:, :, pl.ds(0, n_y * width)], send=3)
    whole(core_buf, send=4)
    whole(y_out.at[pl.ds(0, n_y - 1)], send=5)
    whole(gate_buf.at[pl.ds(0, n_tp - 1)], send=7)
    whole(gate_back.at[pl.ds(0, others)], send=8)
    whole(square_buf.at[pl.ds(0, n_tp - 1)], send=9)

    own_back.wait()
    whole(back_ref.at[part_slots], recv=1)
    token_out[...] = matmul_tn(table_ref[...], back_ref[...]) + matmul_tn(
        signal, router_ref[:, cols(tp)]
    )
    whole(term_buf.at[pl.ds(0, others)], recv=5)
    term_total = term_buf[0]
    for e in range(1, n_ep):
        term_total = term_total + term_buf[e]
    term_out[...] = term_total
    whole(square_buf.at[pl.ds(0, n_tp - 1)], recv=4)
    square = square_buf[0]
    for r in range(1, n_tp):
        square = square + square_buf[r]
    square = square / (hidden * n_tp)
    gate_square_out[...] = square[0:1, :]
    up_square_out[...] = square[1:2, :]

    whole(back_ref.at[part_slots], send=6)
    whole(term_buf.at[pl.ds(0, others)], send=10)


def batches_of(groups):
    if groups == 4:
        return ((0, 2), (2, 1), (3, 1)), ((0, 2), (2, 2))
    single = tuple((j, 1) for j in range(groups))
    return single, single


def layer(routes, weights, tokens, cotangent, router_rows, gate, up, down, n_ep, n_tp, cap):
    tok, width = tokens.shape
    features, hidden = gate.shape[1:]
    chunks = n_ep if n_ep <= 8 else next(c for c in range(8, 0, -1) if n_ep % c == 0)
    size = 2 if chunks % 2 == 0 else 1
    n_y = n_tp // 2
    slots = n_ep * cap
    batches, backs = batches_of(chunks // size)
    batch_rows = slots // chunks * size * max(count for _, count in batches)
    dma = pltpu.SemaphoreType.DMA
    in_vmem = pl.BlockSpec(memory_space=VMEM)
    in_hbm = pl.BlockSpec(memory_space=pltpu.HBM)
    return pl.pallas_call(
        functools.partial(layer_kernel, n_ep, n_tp, chunks, cap),
        out_shape=(
            VMEM((tok, width), F32),
            VMEM(routes.shape, F32),
            VMEM((1, width), F32),
            VMEM((1, features), F32),
            VMEM((1, features), F32),
            VMEM((1, hidden), F32),
            VMEM(gate.shape, BF16),
            VMEM(up.shape, BF16),
            VMEM(down.shape, BF16),
        ),
        in_specs=[in_hbm] * 8,
        out_specs=[in_vmem] * 9,
        scratch_shapes=[
            VMEM(routes.shape, routes.dtype),
            VMEM(weights.shape, BF16),
            VMEM(tokens.shape, BF16),
            VMEM(tokens.shape, BF16),
            VMEM(router_rows.shape, BF16),
            VMEM((features, hidden), BF16),
            VMEM((features, hidden), BF16),
            VMEM((hidden, features), BF16),
            VMEM((hidden, features), BF16),
            VMEM((hidden, features), BF16),
            VMEM((features, hidden), BF16),
            VMEM((slots, tok), BF16),
            VMEM((2, slots, width), BF16),
            VMEM((n_ep, 8, 128), F32),
            VMEM((2, slots, features), BF16),
            VMEM((n_ep, 8, 128), F32),
            VMEM((batch_rows, hidden), F32),
            VMEM((batch_rows, hidden), F32),
            VMEM((batch_rows, hidden), F32),
            VMEM((batch_rows, 128), F32),
            VMEM((batch_rows, 128), F32),
            VMEM((slots, hidden), BF16),
            VMEM((slots, hidden), BF16),
            VMEM((slots, hidden), BF16),
            VMEM((slots, features), BF16),
            VMEM((n_ep, 8, 128), F32),
            VMEM((n_tp, n_ep, 8, 128), F32),
            VMEM((n_ep, 8, 128), F32),
            VMEM((n_ep, 8, 128), F32),
            VMEM((n_y, slots, width), BF16),
            VMEM((n_y, slots, width), BF16),
            VMEM((n_y, slots, width), BF16),
            VMEM((slots, width), BF16),
            VMEM((slots, width), BF16),
            VMEM((n_tp, 2, features), F32),
            VMEM((n_ep, 1, width), F32),
            VMEM((n_ep, 1, width), F32),
            dma((8,)),
            dma((3,)),
            dma((11,)),
            dma((6,)),
            dma((n_ep,)),
            dma((n_y - 1, chunks)),
            dma((n_y, len(batches))),
            dma((n_y, len(backs))),
            dma((n_y - 1, chunks)),
        ],
        compiler_params=pltpu.CompilerParams(
            collective_id=0, has_side_effects=True, vmem_limit_bytes=48 * 2**20
        ),
        name="layer",
    )(routes, weights, tokens, cotangent, router_rows, gate, up, down)


def write_kernel(count, *refs):
    ins, outs, sems = refs[:count], refs[count : 2 * count], refs[-1]
    copies = [
        pltpu.make_async_copy(source, target, sems.at[i])
        for i, (source, target) in enumerate(zip(ins, outs, strict=True))
    ]
    for copy in copies:
        copy.start()
    for copy in copies:
        copy.wait()


def write_out(*arrays):
    count = len(arrays)
    return pl.pallas_call(
        functools.partial(write_kernel, count),
        out_shape=tuple(jax.ShapeDtypeStruct(a.shape, a.dtype) for a in arrays),
        in_specs=[pl.BlockSpec(memory_space=VMEM)] * count,
        out_specs=[pl.BlockSpec(memory_space=pltpu.HBM)] * count,
        scratch_shapes=[pltpu.SemaphoreType.DMA((count,))],
        compiler_params=pltpu.CompilerParams(vmem_limit_bytes=2**20),
        name="write_out",
    )(*(pltpu.with_memory_space_constraint(a, VMEM) for a in arrays))


def shards(tokens, routing, gate_weights, cotangent, expert_gate, expert_up, expert_down, router):
    tok_rows = tokens.shape[0]
    top_count = routing.shape[1]
    experts = router.shape[1]
    n_tp = lax.axis_size("tp")
    n_ep = lax.axis_size("ep")
    capacity = 3 * top_count * tok_rows // (2 * experts)
    results = layer(
        routing.T,
        gate_weights.T,
        tokens,
        cotangent,
        router.T,
        expert_gate,
        expert_up,
        expert_down,
        n_ep,
        n_tp,
        capacity,
    )
    token_grad, gate_grad, router_grad, gate_square, up_square, down_square, gates, ups, downs = (
        write_out(*results)
    )
    return (
        token_grad,
        gate_grad.T,
        gates,
        ups,
        downs,
        router_grad,
        gate_square,
        up_square,
        down_square,
    )


def solution(mesh):
    in_specs = (
        P("ep", "tp"),
        P("ep", None),
        P("ep", None),
        P("ep", "tp"),
        P("ep", None, "tp"),
        P("ep", None, "tp"),
        P("ep", "tp", None),
        P(),
    )
    out_specs = (
        P("ep", "tp"),
        P("ep", None),
        P("ep", None, "tp"),
        P("ep", None, "tp"),
        P("ep", "tp", None),
        P("ep", "tp"),
        P("ep", None),
        P("ep", None),
        P("ep", "tp"),
    )
    return jax.shard_map(shards, mesh=mesh, in_specs=in_specs, out_specs=out_specs, check_vma=False)
```

time: 69.8 us -> 54.5 us (0.78)
  Pallas kernels: 68.4 us -> 53.7 us
    pallas_call x1, Pallas kernels: 64.5 us -> 49.7 us  [layer(): pl.pallas_call(functools.partial(layer_kernel, n_ep, n_tp, chunks, cap),...]
where the time goes in v2:
time: 54.5 us; the launch traced here: 54.3 us
  Pallas kernels  53.7 us (99%)
  between operations  0.65 us (1%)
    pallas_call x1, Pallas kernels, layer(): pl.pallas_call(functools.partial(layer_kernel, n_ep, n_tp, chunks, cap),...  49.7 us
    pallas_call x1, Pallas kernels, write_out(): pl.pallas_call(functools.partial(write_kernel, count), out_shape=tuple((j...  3.93 us

profile of v2, /device:TPU:0, one launch (start us, length us, event | category | flops | bytes accessed | tf_op | source)
XLA Modules:
  0.0 54.3 jit_solution(6944279393717460301)
XLA Ops:
  0.6 49.7 %layer.1 = (f32[128,512]{1,0:T(8,128)S(1)}, f32[2,128]{1,0:T(2,128)S(1)}, f32[1,512]{1,0:T(1,128)S(1)}, f32[1,2048]{1,0:T(1,128)S(1)}, f32[1,2048]{1,0:T(1,128)S...) custom-call(s32[2,128]{1,0:T(2,128)} %bitcast.5, ...), custom_call_target="tpu_custom_call" | custom-call | tf_op jit(solution)/shard_map/layer/pallas_call | solution.py:730
  50.4 3.9 %write_out.1 = (f32[128,512]{1,0:T(8,128)}, f32[2,128]{1,0:T(2,128)}, f32[1,512]{1,0:T(1,128)}, f32[1,2048]{1,0:T(1,128)}, f32[1,2048]{1,0:T(1,128)}, /*index=5*...) custom-call(f32[128,512]{1,0:T(8,128)S(1)} %get-tuple-element.27.refs_0_,, ...), custom_call_target="tpu_custom_call" | custom-call | tf_op jit(solution)/shard_map/write_out/pallas_call | solution.py:814

commit v3 on v2

--- a/solution.py
+++ b/solution.py
@@ -111,7 +111,8 @@
         out_ref[which] = matmul_nn(table, source[...]).astype(BF16)
     spread = matmul_nt(chosen.astype(BF16), table) * own_block(n_ep, cap)
     values = matmul_nn(spread.astype(BF16), lane_pick(n_ep, cap).astype(BF16))
-    w_ref[...] = jnp.broadcast_to(values[:, None, :], w_ref.shape)
+    for e in range(n_ep):
+        w_ref[e] = values[e : e + 1, :]
 
 
 def layer_kernel(
@@ -123,31 +124,29 @@
     weights_hbm,
     tokens_hbm,
     cotangent_hbm,
-    router_hbm,
     gate_hbm,
     up_hbm,
     down_hbm,
-    token_out,
-    gate_out,
-    term_out,
-    gate_square_out,
-    up_square_out,
-    down_square_out,
     gate_res,
     up_res,
     down_res,
+    back_ref,
+    table_ref,
+    signal_out,
+    term_buf,
+    square_buf,
+    gate_out,
+    down_square_out,
     routes_ref,
     weights_ref,
     tokens_ref,
     cotangent_ref,
-    router_ref,
     gate_w,
     up_w,
     down_w,
     gate_t,
     up_t,
     down_t,
-    table_ref,
     slots_ref,
     w_ref,
     full_ref,
@@ -169,10 +168,7 @@
     y_out,
     y_buf,
     ep_out,
-    back_ref,
-    square_buf,
     term_ref,
-    term_buf,
     load_sem,
     own_sem,
     send_sem,
@@ -197,7 +193,7 @@
     group_rows = size * rows
     exact_rows = 16 if group_rows % 16 == 0 else 8
 
-    batches, backs = batches_of(groups)
+    batches = batches_of(groups)
 
     def cols(which):
         return pl.ds(pl.multiple_of(which * width, width), width)
@@ -239,27 +235,27 @@
     def chunk_at(j, i):
         return group_at(j) * size + paired(lax.rem(lax.div(ep, per), size), i, size)
 
-    def ep_copy(dst, src):
+    def ep_copy(dst, src, part):
         return remote(
-            slots_ref.at[:, source_rows(dst), :],
-            full_ref.at[:, source_rows(src), cols(tp)],
+            slots_ref.at[part, source_rows(dst), :],
+            full_ref.at[part, source_rows(src), cols(tp)],
             send_sem.at[0],
-            ep_recv.at[src],
+            ep_recv.at[part, src],
             (dst, tp),
         )
 
     def w_copy(dst, src):
         return remote(w_ref.at[dst], full_w_ref.at[src], send_sem.at[1], all_recv.at[0], (dst, tp))
 
-    def y_copy(source_y, target_y, chunk, r):
-        piece = full_ref.at[:, chunk_rows(chunk), cols(source_y * 2 + core)]
+    def y_copy(source_y, target_y, chunk, r, part):
+        piece = full_ref.at[part, chunk_rows(chunk), cols(source_y * 2 + core)]
         return remote(
-            piece, piece, send_sem.at[2], y_recv.at[r - 1, chunk], (ep, target_y * 2 + core)
-        )
-
-    def core_copy(source_y, source_core, at, slot, batch):
-        piece = full_ref.at[:, at, cols(source_y * 2 + source_core)]
-        return remote(piece, piece, send_sem.at[3], core_recv.at[slot, batch], (ep, partner))
+            piece, piece, send_sem.at[2], y_recv.at[r - 1, part, chunk], (ep, target_y * 2 + core)
+        )
+
+    def core_copy(source_y, source_core, at, slot, batch, part):
+        piece = full_ref.at[part, at, cols(source_y * 2 + source_core)]
+        return remote(piece, piece, send_sem.at[3], core_recv.at[slot, part, batch], (ep, partner))
 
     def rcore_copy(target_y, j, count, slot, back):
         at = group_range(j, count)
@@ -332,7 +328,6 @@
         (gate_hbm.at[0], gate_w),
         (up_hbm.at[0], up_w),
         (down_hbm.at[0], down_w),
-        (router_hbm, router_ref),
     )
     loads = [pltpu.make_async_copy(*pair, load_sem.at[i]) for i, pair in enumerate(pairs)]
 
@@ -379,7 +374,8 @@
 
     def send_group(j):
         for i in range(size):
-            each_source(j, i, lambda dst: ep_copy(dst, ep).start())
+            for part in range(2):
+                each_source(j, i, lambda dst: ep_copy(dst, ep, part).start())
 
     loop(1, n_ep, lambda r: w_copy(lax.rem(ep + r, n_ep), ep).start())
     loop(0, groups, send_group)
@@ -392,47 +388,44 @@
 
     def relay(j, i):
         chunk = chunk_at(j, i)
-        each_source(j, i, lambda source: ep_copy(ep, source).wait_recv())
-        for r in range(1, n_y):
-            y_copy(y, lax.rem(y + r, n_y), chunk, r).start()
-        core_copy(y, core, chunk_rows(chunk), 0, batch_of(j)).start()
+        for part in range(2):
+            each_source(j, i, lambda source: ep_copy(ep, source, part).wait_recv())
+            for r in range(1, n_y):
+                y_copy(y, lax.rem(y + r, n_y), chunk, r, part).start()
+            core_copy(y, core, chunk_rows(chunk), 0, batch_of(j), part).start()
 
     def forward(j, i):
         chunk = chunk_at(j, i)
-        for r in range(1, n_y):
-            source_y = lax.rem(y + n_y - r, n_y)
-            y_copy(source_y, y, chunk, r).wait_recv()
-            core_copy(source_y, core, chunk_rows(chunk), r, batch_of(j)).start()
+        for part in range(2):
+            for r in range(1, n_y):
+                source_y = lax.rem(y + n_y - r, n_y)
+                y_copy(source_y, y, chunk, r, part).wait_recv()
+                core_copy(source_y, core, chunk_rows(chunk), r, batch_of(j), part).start()
 
     def chunks_of(batch):
         j, count = batches[batch]
         return [(k, i) for k in range(j, j + count) for i in range(size)]
 
-    def back_chunks(back):
-        j, count = backs[back]
-        return [(k, i) for k in range(j, j + count) for i in range(size)]
-
-    def multiply(batch, which, first):
+    def product(batch, source_y, slot):
         at = batch_rows(batch)
         many = batches[batch][1] * group_rows
-        k = y_cols(which)
-        x, t = full_ref[0, at, k], full_ref[1, at, k]
-        for out, value in (
-            (pre_gate, matmul_nn(x, gate_w[k, :])),
-            (pre_up, matmul_nn(x, up_w[k, :])),
-            (back_proj, matmul_nn(t, down_t[k, :])),
-        ):
-            out[0:many, :] = value if first else out[0:many, :] + value
+        k = y_cols(source_y)
+
+        def put(out, value):
+            out[0:many, :] = value if slot == 0 else out[0:many, :] + value
+
+        core_copy(source_y, 1 - core, at, slot, batch, 0).wait_recv()
+        put(pre_gate, matmul_nn(full_ref[0, at, k], gate_w[k, :]))
+        put(pre_up, matmul_nn(full_ref[0, at, k], up_w[k, :]))
+        core_copy(source_y, 1 - core, at, slot, batch, 1).wait_recv()
+        put(back_proj, matmul_nn(full_ref[1, at, k], down_t[k, :]))
 
     def near_product(batch):
-        core_copy(y, 1 - core, batch_rows(batch), 0, batch).wait_recv()
-        multiply(batch, y, True)
+        product(batch, y, 0)
 
     def far_product(batch):
         for r in range(1, n_y):
-            source_y = lax.rem(y + n_y - r, n_y)
-            core_copy(source_y, 1 - core, batch_rows(batch), r, batch).wait_recv()
-            multiply(batch, source_y, False)
+            product(batch, lax.rem(y + n_y - r, n_y), r)
 
     part_cols = 256 if hidden % 256 == 0 else hidden
     lane_sums = part_cols % 128 == 0
@@ -442,7 +435,7 @@
         first = base_of(*batches[batch]) * (size * per)
         many = batches[batch][1] * size * per
         for n in range(many):
-            weight = jnp.broadcast_to(full_w_ref[first + n][0:1, :], (128, 128)).T
+            weight = jnp.broadcast_to(full_w_ref[first + n], (128, 128)).T
             slot_w[n * cap : (n + 1) * cap, :] = weight[0:cap, :]
         for b in range(0, many * cap, exact_rows):
             here = slice(b, b + exact_rows)
@@ -476,10 +469,10 @@
         for n in range(many):
             column = slot_sum[n * cap : (n + 1) * cap, :]
             block_sum = jnp.concatenate([column, jnp.zeros((128 - cap, 128), F32)], axis=0)
-            gate_send_ref[first + n] = jnp.broadcast_to(block_sum.T[0:1, :], (8, 128))
+            gate_send_ref[first + n] = block_sum.T[0:1, :]
 
     def slot_grads(back, r, own):
-        j, count = backs[back]
+        j, count = batches[back]
         at = group_range(j, count)
         target = lax.rem(y + r, n_y)
         block = cols(target * 2 + (core if own else 1 - core))
@@ -489,19 +482,21 @@
         if not own:
             rcore_copy(target, j, count, r, back).start()
 
-    def across(back):
+    def across_arrives(back):
+        for r in range(1, n_y):
+            rcore_copy(lax.rem(y + r, n_y), *batches[back], r, back).wait_recv()
+
+    def across(j, i):
+        chunk = chunk_at(j, i)
+        here = chunk_rows(chunk)
         for r in range(1, n_y):
             target = lax.rem(y + r, n_y)
-            rcore_copy(target, *backs[back], r, back).wait_recv()
-            for j, i in back_chunks(back):
-                chunk = chunk_at(j, i)
-                here = chunk_rows(chunk)
-                mine = part_ref[here, cols(target * 2 + core)].astype(F32)
-                y_out[target, here] = (mine + core_buf[target, here].astype(F32)).astype(BF16)
-                ry_copy(y, target, chunk, r).start()
+            mine = part_ref[here, cols(target * 2 + core)].astype(F32)
+            y_out[target, here] = (mine + core_buf[target, here].astype(F32)).astype(BF16)
+            ry_copy(y, target, chunk, r).start()
 
     def own_arrives(back):
-        rcore_copy(y, *backs[back], 0, back).wait_recv()
+        rcore_copy(y, *batches[back], 0, back).wait_recv()
 
     def scatter(j, i):
         chunk = chunk_at(j, i)
@@ -514,9 +509,6 @@
         ep_out[here, :] = value.astype(BF16)
         each_source(j, i, lambda dst: rep_copy(dst, ep).start())
 
-    for load in loads[4:]:
-        load.wait()
-
     def each(chosen, body):
         for j, i in chosen:
             body(j, i)
@@ -528,62 +520,28 @@
 
     def slots_own(back):
         slot_grads(back, 0, False)
-        across(back)
         slot_grads(back, 0, True)
 
     def prep_tile(source, target, turns):
         def turn(i, carry):
-            span = pl.ds(pl.multiple_of(i * 256, 256), 256)
+            span = pl.ds(pl.multiple_of(i * block_rows, block_rows), block_rows)
             target[:, span] = source[span, :].T
             return carry
 
         lax.fori_loop(0, turns, turn, 0)
 
+    block_rows = 256 if features % 256 == 0 else features
+    blocks = features // block_rows
+
     def prep_down():
-        span = 256 if hidden % 256 == 0 else hidden
-        for c in range(0, hidden, span):
-            down_t[:, c : c + span] = down_w[c : c + span, :].T
-
-    prep_down()
-    last = len(batches) - 1
-    ready = {k + count - 1: b for b, (k, count) in enumerate(backs)}
-    each(chunks_of(0)[:2], relay)
-    prep_tile(gate_w, gate_t, features // 256)
-    each(chunks_of(0)[2:], relay)
-    prep_tile(up_w, up_t, features // 256)
-    near_product(0)
-    whole(full_w_ref.at[pl.ds(0, others)], recv=0)
-    pending = None
-    for b in range(last):
-        later = chunks_of(b + 1)
-        if b == 0:
-            each(later[:1], relay)
-            each(chunks_of(0), forward)
-            each(later[1:], relay)
-        far_product(b)
-        gradients(b)
-        near_product(b + 1)
-        after = chunks_of(b + 2) if b + 2 <= last else []
-        each(after[:1], relay)
-        each(later, forward)
-        if pending is not None:
-            slots_own(pending)
-            pending = None
-        done = ready.get(sum(batches[b]) - 1)
-        if done is not None:
-            slots_other(done)
-            pending = done
-        each(after[1:], relay)
-    if pending is not None:
-        slots_own(pending)
-    if last == 0:
-        each(chunks_of(0), forward)
-    far_product(last)
-    gradients(last)
-    loop(1, n_tp, lambda r: tp_copy(lax.rem(tp + r, n_tp), tp).start())
-    gate_buf[tp] = gate_send_ref[...]
-    final = len(backs) - 1
-    slots_other(final)
+        for c in range(0, hidden, part_cols):
+            down_t[:, c : c + part_cols] = down_w[c : c + part_cols, :].T
+
+    final = len(batches) - 1
+
+    def send_gates():
+        loop(1, n_tp, lambda r: tp_copy(lax.rem(tp + r, n_tp), tp).start())
+        gate_buf[tp] = gate_send_ref[...]
 
     def add_gates():
         whole(gate_buf.at[pl.ds(0, n_tp - 1)], recv=2)
@@ -594,9 +552,66 @@
         loop(1, n_ep, lambda r: gate_copy(lax.rem(ep + r, n_ep), ep).start())
         gate_back[ep] = gate_back_out[ep]
 
-    slots_own(final)
-
-    tile = 256 if features % 256 == 0 else features
+    first = chunks_of(0)
+    half = (len(first) + 1) // 2
+    each(first[:1], relay)
+    for load in loads[4:]:
+        load.wait()
+    prep_down()
+    each(first[1:half], relay)
+    prep_tile(gate_w, gate_t, blocks)
+    each(first[half:], relay)
+    prep_tile(up_w, up_t, blocks)
+    near_product(0)
+    whole(full_w_ref.at[pl.ds(0, others)], recv=0)
+    if final == 2:
+        second, third = chunks_of(1), chunks_of(2)
+        each(second[:1], relay)
+        each(first, forward)
+        each(second[1:], relay)
+        far_product(0)
+        gradients(0)
+        slots_other(0)
+        each(third[:1], relay)
+        each(second, forward)
+        near_product(1)
+        each(third[1:], relay)
+        far_product(1)
+        gradients(1)
+        slots_other(1)
+        slots_own(1)
+        across_arrives(1)
+        each(second, across)
+        near_product(2)
+        each(third, forward)
+        slots_own(0)
+        across_arrives(0)
+        each(first[:half], across)
+        far_product(2)
+        gradients(2)
+        send_gates()
+        slots_other(2)
+        each(first[half:], across)
+        own_arrives(1)
+        each(second, scatter)
+        slots_own(2)
+        across_arrives(2)
+        each(third, across)
+    else:
+        for b in range(final + 1):
+            if b > 0:
+                each(chunks_of(b), relay)
+                near_product(b)
+            each(chunks_of(b), forward)
+            far_product(b)
+            gradients(b)
+            slots_other(b)
+            slots_own(b)
+            across_arrives(b)
+            each(chunks_of(b), across)
+        send_gates()
+
+    tile = 512 if features % 512 == 0 else features
     tiles = features // tile
 
     def gate_tile(i, carry):
@@ -619,25 +634,30 @@
         square = jnp.sum(total * total, axis=1, keepdims=True)
         down_square_out[0:1, span] = jnp.broadcast_to(square, (down_tile, 128)).T[0:1, :] / features
 
-    early = min(2, tiles)
-    middle = min(tiles, early + 2)
-    chosen = back_chunks(final)
-    half = (len(chosen) + 1) // 2
+    def tiles_to(first, end):
+        lax.fori_loop(min(first, tiles), min(end, tiles), gate_tile, 0)
+
+    tiles_to(0, 1)
+    add_gates()
+    tiles_to(1, 2)
     for b in range(final):
-        own_arrives(b)
-        each(back_chunks(b), scatter)
-    lax.fori_loop(0, 1, gate_tile, 0)
-    add_gates()
-    lax.fori_loop(1, early, gate_tile, 0)
+        if final != 2 or b != 1:
+            own_arrives(b)
+            each(chunks_of(b), scatter)
     own_arrives(final)
-    each(chosen[:half], scatter)
-    lax.fori_loop(early, middle, gate_tile, 0)
+    each(chunks_of(final)[:1], scatter)
+    tiles_to(2, 3)
+    each(chunks_of(final)[1:], scatter)
+    own_back = pltpu.make_async_copy(
+        ep_out.at[source_rows(ep)], back_ref.at[source_rows(ep)], own_sem.at[2]
+    )
+    own_back.start()
 
     whole(gate_back.at[pl.ds(0, others)], recv=3)
     routes = routes_ref[...]
     weights = weights_ref[...].astype(F32)
     labels = lax.broadcasted_iota(jnp.int32, (n_ep, tok), 0)
-    rest = gate_back[:, 0, :]
+    rest = jnp.concatenate([gate_back[e] for e in range(n_ep)], axis=0)
     pieces = []
     for _ in range(3):
         pieces.append(rest.astype(BF16).astype(F32))
@@ -664,14 +684,10 @@
     term = matmul_nn(signal, tokens_ref[...])
     for e in range(n_ep):
         term_ref[e] = term[e : e + 1, :]
+    signal_out[...] = signal
     loop(1, n_ep, lambda r: term_copy(lax.rem(ep + r, n_ep), ep).start())
     term_buf[ep] = term_ref[ep]
-    each(chosen[half:], scatter)
-    own_back = pltpu.make_async_copy(
-        ep_out.at[source_rows(ep)], back_ref.at[source_rows(ep)], own_sem.at[2]
-    )
-    own_back.start()
-    lax.fori_loop(middle, tiles, gate_tile, 0)
+    tiles_to(3, tiles)
     loop(1, n_tp, lambda r: square_copy(lax.rem(tp + r, n_tp), tp).start())
     for i in range(hidden // down_tile):
         down_part(i)
@@ -688,41 +704,26 @@
 
     own_back.wait()
     whole(back_ref.at[part_slots], recv=1)
-    token_out[...] = matmul_tn(table_ref[...], back_ref[...]) + matmul_tn(
-        signal, router_ref[:, cols(tp)]
-    )
     whole(term_buf.at[pl.ds(0, others)], recv=5)
-    term_total = term_buf[0]
-    for e in range(1, n_ep):
-        term_total = term_total + term_buf[e]
-    term_out[...] = term_total
     whole(square_buf.at[pl.ds(0, n_tp - 1)], recv=4)
-    square = square_buf[0]
-    for r in range(1, n_tp):
-        square = square + square_buf[r]
-    square = square / (hidden * n_tp)
-    gate_square_out[...] = square[0:1, :]
-    up_square_out[...] = square[1:2, :]
-
     whole(back_ref.at[part_slots], send=6)
     whole(term_buf.at[pl.ds(0, others)], send=10)
 
 
 def batches_of(groups):
     if groups == 4:
-        return ((0, 2), (2, 1), (3, 1)), ((0, 2), (2, 2))
-    single = tuple((j, 1) for j in range(groups))
-    return single, single
-
-
-def layer(routes, weights, tokens, cotangent, router_rows, gate, up, down, n_ep, n_tp, cap):
+        return ((0, 2), (2, 1), (3, 1))
+    return tuple((j, 1) for j in range(groups))
+
+
+def layer(routes, weights, tokens, cotangent, gate, up, down, n_ep, n_tp, cap):
     tok, width = tokens.shape
     features, hidden = gate.shape[1:]
     chunks = n_ep if n_ep <= 8 else next(c for c in range(8, 0, -1) if n_ep % c == 0)
     size = 2 if chunks % 2 == 0 else 1
     n_y = n_tp // 2
     slots = n_ep * cap
-    batches, backs = batches_of(chunks // size)
+    batches = batches_of(chunks // size)
     batch_rows = slots // chunks * size * max(count for _, count in batches)
     dma = pltpu.SemaphoreType.DMA
     in_vmem = pl.BlockSpec(memory_space=VMEM)
@@ -730,35 +731,34 @@
     return pl.pallas_call(
         functools.partial(layer_kernel, n_ep, n_tp, chunks, cap),
         out_shape=(
-            VMEM((tok, width), F32),
-            VMEM(routes.shape, F32),
-            VMEM((1, width), F32),
-            VMEM((1, features), F32),
-            VMEM((1, features), F32),
-            VMEM((1, hidden), F32),
             VMEM(gate.shape, BF16),
             VMEM(up.shape, BF16),
             VMEM(down.shape, BF16),
+            VMEM((slots, width), BF16),
+            VMEM((slots, tok), BF16),
+            VMEM((n_ep, tok), BF16),
+            VMEM((n_ep, 1, width), F32),
+            VMEM((n_tp, 2, features), F32),
+            VMEM(routes.shape, F32),
+            VMEM((1, hidden), F32),
         ),
-        in_specs=[in_hbm] * 8,
-        out_specs=[in_vmem] * 9,
+        in_specs=[in_hbm] * 7,
+        out_specs=[in_vmem] * 10,
         scratch_shapes=[
             VMEM(routes.shape, routes.dtype),
             VMEM(weights.shape, BF16),
             VMEM(tokens.shape, BF16),
             VMEM(tokens.shape, BF16),
-            VMEM(router_rows.shape, BF16),
             VMEM((features, hidden), BF16),
             VMEM((features, hidden), BF16),
             VMEM((hidden, features), BF16),
             VMEM((hidden, features), BF16),
             VMEM((hidden, features), BF16),
             VMEM((features, hidden), BF16),
-            VMEM((slots, tok), BF16),
             VMEM((2, slots, width), BF16),
-            VMEM((n_ep, 8, 128), F32),
+            VMEM((n_ep, 1, 128), F32),
             VMEM((2, slots, features), BF16),
-            VMEM((n_ep, 8, 128), F32),
+            VMEM((n_ep, 1, 128), F32),
             VMEM((batch_rows, hidden), F32),
             VMEM((batch_rows, hidden), F32),
             VMEM((batch_rows, hidden), F32),
@@ -768,58 +768,132 @@
             VMEM((slots, hidden), BF16),
             VMEM((slots, hidden), BF16),
             VMEM((slots, features), BF16),
-            VMEM((n_ep, 8, 128), F32),
-            VMEM((n_tp, n_ep, 8, 128), F32),
-            VMEM((n_ep, 8, 128), F32),
-            VMEM((n_ep, 8, 128), F32),
+            VMEM((n_ep, 1, 128), F32),
+            VMEM((n_tp, n_ep, 1, 128), F32),
+            VMEM((n_ep, 1, 128), F32),
+            VMEM((n_ep, 1, 128), F32),
             VMEM((n_y, slots, width), BF16),
             VMEM((n_y, slots, width), BF16),
             VMEM((n_y, slots, width), BF16),
             VMEM((slots, width), BF16),
-            VMEM((slots, width), BF16),
-            VMEM((n_tp, 2, features), F32),
             VMEM((n_ep, 1, width), F32),
-            VMEM((n_ep, 1, width), F32),
-            dma((8,)),
+            dma((7,)),
             dma((3,)),
             dma((11,)),
             dma((6,)),
-            dma((n_ep,)),
-            dma((n_y - 1, chunks)),
+            dma((2, n_ep)),
+            dma((n_y - 1, 2, chunks)),
+            dma((n_y, 2, len(batches))),
             dma((n_y, len(batches))),
-            dma((n_y, len(backs))),
             dma((n_y - 1, chunks)),
         ],
         compiler_params=pltpu.CompilerParams(
             collective_id=0, has_side_effects=True, vmem_limit_bytes=48 * 2**20
         ),
         name="layer",
-    )(routes, weights, tokens, cotangent, router_rows, gate, up, down)
-
-
-def write_kernel(count, *refs):
-    ins, outs, sems = refs[:count], refs[count : 2 * count], refs[-1]
-    copies = [
-        pltpu.make_async_copy(source, target, sems.at[i])
-        for i, (source, target) in enumerate(zip(ins, outs, strict=True))
-    ]
-    for copy in copies:
+    )(routes, weights, tokens, cotangent, gate, up, down)
+
+
+def finish_kernel(
+    hidden,
+    gate_ref,
+    up_ref,
+    down_ref,
+    back_ref,
+    table_ref,
+    signal_ref,
+    term_buf,
+    square_buf,
+    gate_grad_ref,
+    down_square_ref,
+    router_hbm,
+    gate_out,
+    up_out,
+    down_out,
+    token_out,
+    gate_grad_out,
+    term_out,
+    gate_square_out,
+    up_square_out,
+    down_square_out,
+    router_ref,
+    token_ref,
+    term_ref,
+    gate_square_ref,
+    up_square_ref,
+    sems,
+):
+    tp = lax.axis_index("tp")
+    n_ep, _, width = term_buf.shape
+    load = pltpu.make_async_copy(router_hbm, router_ref, sems.at[0])
+    load.start()
+    pairs = (
+        (gate_ref, gate_out),
+        (up_ref, up_out),
+        (down_ref, down_out),
+        (gate_grad_ref, gate_grad_out),
+        (down_square_ref, down_square_out),
+        (term_ref, term_out),
+        (gate_square_ref, gate_square_out),
+        (up_square_ref, up_square_out),
+        (token_ref, token_out),
+    )
+    copies = [pltpu.make_async_copy(*pair, sems.at[i + 1]) for i, pair in enumerate(pairs)]
+    for copy in copies[:5]:
         copy.start()
+    term = term_buf[0]
+    for e in range(1, n_ep):
+        term = term + term_buf[e]
+    term_ref[...] = term
+    square = square_buf[0]
+    for r in range(1, square_buf.shape[0]):
+        square = square + square_buf[r]
+    square = square / hidden
+    gate_square_ref[...] = square[0:1, :]
+    up_square_ref[...] = square[1:2, :]
+    for copy in copies[5:8]:
+        copy.start()
+    token = matmul_tn(table_ref[...], back_ref[...])
+    load.wait()
+    cols = pl.ds(pl.multiple_of(tp * width, width), width)
+    token_ref[...] = token + matmul_tn(signal_ref[...], router_ref[:, cols])
+    copies[8].start()
     for copy in copies:
         copy.wait()
 
 
-def write_out(*arrays):
-    count = len(arrays)
+def finish(results, router_rows, hidden):
+    gates, ups, downs, back, _, _, terms, squares, gate_grad, down_square = results
+    tok, width = gate_grad.shape[1], back.shape[1]
+    features = squares.shape[2]
+    outs = (
+        (gates.shape, BF16),
+        (ups.shape, BF16),
+        (downs.shape, BF16),
+        ((tok, width), F32),
+        (gate_grad.shape, F32),
+        (terms.shape[1:], F32),
+        ((1, features), F32),
+        ((1, features), F32),
+        (down_square.shape, F32),
+    )
+    count = len(results)
     return pl.pallas_call(
-        functools.partial(write_kernel, count),
-        out_shape=tuple(jax.ShapeDtypeStruct(a.shape, a.dtype) for a in arrays),
-        in_specs=[pl.BlockSpec(memory_space=VMEM)] * count,
-        out_specs=[pl.BlockSpec(memory_space=pltpu.HBM)] * count,
-        scratch_shapes=[pltpu.SemaphoreType.DMA((count,))],
-        compiler_params=pltpu.CompilerParams(vmem_limit_bytes=2**20),
-        name="write_out",
-    )(*(pltpu.with_memory_space_constraint(a, VMEM) for a in arrays))
+        functools.partial(finish_kernel, hidden),
+        out_shape=tuple(jax.ShapeDtypeStruct(*out) for out in outs),
+        in_specs=[pl.BlockSpec(memory_space=VMEM)] * count + [pl.BlockSpec(memory_space=pltpu.HBM)],
+        out_specs=[pl.BlockSpec(memory_space=pltpu.HBM)] * len(outs),
+        scratch_shapes=[
+            VMEM(router_rows.shape, BF16),
+            VMEM((tok, width), F32),
+            VMEM((1, width), F32),
+            VMEM((1, features), F32),
+            VMEM((1, features), F32),
+            pltpu.SemaphoreType.DMA((10,)),
+        ],
+        compiler_params=pltpu.CompilerParams(vmem_limit_bytes=4 * 2**20),
+        name="finish",
+    )(*(pltpu.with_memory_space_constraint(a, VMEM) for a in results), router_rows)
 
 
 def shards(tokens, routing, gate_weights, cotangent, expert_gate, expert_up, expert_down, router):
@@ -834,7 +908,6 @@
         gate_weights.T,
         tokens,
         cotangent,
-        router.T,
         expert_gate,
         expert_up,
         expert_down,
@@ -842,8 +915,9 @@
         n_tp,
         capacity,
     )
-    token_grad, gate_grad, router_grad, gate_square, up_square, down_square, gates, ups, downs = (
-        write_out(*results)
+    hidden = expert_gate.shape[2] * n_tp
+    gates, ups, downs, token_grad, gate_grad, router_grad, gate_square, up_square, down_square = (
+        finish(results, router.T, hidden)
     )
     return (
         token_grad,

time: 54.5 us -> 51.2 us (0.939)
  Pallas kernels: 53.7 us -> 50.3 us
    pallas_call x1, Pallas kernels: 49.7 us -> 46.4 us  [layer(): pl.pallas_call(functools.partial(layer_kernel, n_ep, n_tp, chunks, cap),...]
where the time goes in v3:
time: 51.2 us; the launch traced here: 51.1 us
  Pallas kernels  50.3 us (98%)
  between operations  0.83 us (2%)
    pallas_call x1, Pallas kernels, layer(): pl.pallas_call(functools.partial(layer_kernel, n_ep, n_tp, chunks, cap),...  46.4 us
    pallas_call x1, Pallas kernels, finish(): pl.pallas_call(functools.partial(finish_kernel, hidden), out_shape=tuple(...  3.89 us

profile of v3, /device:TPU:0, one launch (start us, length us, event | category | flops | bytes accessed | tf_op | source)
XLA Modules:
  0.0 51.1 jit_solution(8047684928245909925)
XLA Ops:
  0.6 0.0 copy-start
  0.7 46.4 %layer.1 = (bf16[1,2048,768]{2,1,0:T(8,128)(2,1)S(1)}, bf16[1,2048,768]{2,1,0:T(8,128)(2,1)S(1)}, bf16[1,768,2048]{2,1,0:T(8,128)(2,1)S(1)}, bf16[384,512]{1,0:T...) custom-call(s32[2,128]{1,0:T(2,128)} %bitcast.5, ...), custom_call_target="tpu_custom_call" | custom-call | tf_op jit(solution)/shard_map/layer/pallas_call | solution.py:731
  47.0 0.0 copy-done
  47.0 3.9 %finish.1 = (bf16[1,2048,768]{2,1,0:T(8,128)(2,1)}, bf16[1,2048,768]{2,1,0:T(8,128)(2,1)}, bf16[1,768,2048]{2,1,0:T(8,128)(2,1)}, f32[128,512]{1,0:T(8,128)}, f3...) custom-call(bf16[1,2048,768]{2,1,0:T(8,128)(2,1)S(1)} %get-tuple-element.28., ...), custom_call_target="tpu_custom_call" | custom-call | tf_op jit(solution)/shard_map/finish/pallas_call | solution.py:881
Async XLA Ops:
  0.6 46.4 %copy-start = (bf16[2048,8]{0,1:T(8,128)(2,1)S(1)}, bf16[2048,8]{0,1:T(8,128)(2,1)}, u32[]{:S(2)}) copy-start(bf16[2048,8]{0,1:T(8,128)(2,1)} %param.15) | copy-start | bytes 98308

commit v4 on v3

--- a/solution.py
+++ b/solution.py
@@ -247,10 +247,10 @@
     def w_copy(dst, src):
         return remote(w_ref.at[dst], full_w_ref.at[src], send_sem.at[1], all_recv.at[0], (dst, tp))
 
-    def y_copy(source_y, target_y, chunk, r, part):
-        piece = full_ref.at[part, chunk_rows(chunk), cols(source_y * 2 + core)]
+    def y_copy(source_y, target_y, at, slot, r, part):
+        piece = full_ref.at[part, at, cols(source_y * 2 + core)]
         return remote(
-            piece, piece, send_sem.at[2], y_recv.at[r - 1, part, chunk], (ep, target_y * 2 + core)
+            piece, piece, send_sem.at[2], y_recv.at[r - 1, part, slot], (ep, target_y * 2 + core)
         )
 
     def core_copy(source_y, source_core, at, slot, batch, part):
@@ -386,12 +386,16 @@
     def batch_of(j):
         return next(b for b, (k, count) in enumerate(batches) if k <= j < k + count)
 
+    def y_slot(j, i):
+        return max(0, (j - batches[0][1]) * size + i + 1) if j >= batches[0][1] else 0
+
     def relay(j, i):
         chunk = chunk_at(j, i)
         for part in range(2):
             each_source(j, i, lambda source: ep_copy(ep, source, part).wait_recv())
             for r in range(1, n_y):
-                y_copy(y, lax.rem(y + r, n_y), chunk, r, part).start()
+                at = chunk_rows(chunk)
+                y_copy(y, lax.rem(y + r, n_y), at, y_slot(j, i), r, part).start()
             core_copy(y, core, chunk_rows(chunk), 0, batch_of(j), part).start()
 
     def forward(j, i):
@@ -399,8 +403,17 @@
         for part in range(2):
             for r in range(1, n_y):
                 source_y = lax.rem(y + n_y - r, n_y)
-                y_copy(source_y, y, chunk, r, part).wait_recv()
-                core_copy(source_y, core, chunk_rows(chunk), r, batch_of(j), part).start()
+                at = chunk_rows(chunk)
+                y_copy(source_y, y, at, y_slot(j, i), r, part).wait_recv()
+                core_copy(source_y, core, at, r, batch_of(j), part).start()
+
+    def forward_first():
+        at = batch_rows(0)
+        for part in range(2):
+            for r in range(1, n_y):
+                source_y = lax.rem(y + n_y - r, n_y)
+                y_copy(source_y, y, at, 0, r, part).wait_recv()
+                core_copy(source_y, core, at, r, 0, part).start()
 
     def chunks_of(batch):
         j, count = batches[batch]
@@ -567,7 +580,7 @@
     if final == 2:
         second, third = chunks_of(1), chunks_of(2)
         each(second[:1], relay)
-        each(first, forward)
+        forward_first()
         each(second[1:], relay)
         far_product(0)
         gradients(0)
@@ -602,7 +615,10 @@
             if b > 0:
                 each(chunks_of(b), relay)
                 near_product(b)
-            each(chunks_of(b), forward)
+            if b == 0:
+                forward_first()
+            else:
+                each(chunks_of(b), forward)
             far_product(b)
             gradients(b)
             slots_other(b)
@@ -782,7 +798,7 @@
             dma((11,)),
             dma((6,)),
             dma((2, n_ep)),
-            dma((n_y - 1, 2, chunks)),
+            dma((n_y - 1, 2, chunks - batches[0][1] * size + 1)),
             dma((n_y, 2, len(batches))),
             dma((n_y, len(batches))),
             dma((n_y - 1, chunks)),

time: 51.2 us -> 51.2 us (level)
  no operation moved by 1% of the time
where the time goes in v4:
time: 51.2 us; the launch traced here: 51.1 us
  Pallas kernels  50.2 us (98%)
  between operations  0.83 us (2%)
    pallas_call x1, Pallas kernels, layer(): pl.pallas_call(functools.partial(layer_kernel, n_ep, n_tp, chunks, cap),...  46.3 us
    pallas_call x1, Pallas kernels, finish(): pl.pallas_call(functools.partial(finish_kernel, hidden), out_shape=tuple(...  3.89 us

profile of v4, /device:TPU:0, one launch (start us, length us, event | category | flops | bytes accessed | tf_op | source)
XLA Modules:
  0.0 51.1 jit_solution(3735012386563944377)
XLA Ops:
  0.6 0.0 copy-start
  0.7 46.3 %layer.1 = (bf16[1,2048,768]{2,1,0:T(8,128)(2,1)S(1)}, bf16[1,2048,768]{2,1,0:T(8,128)(2,1)S(1)}, bf16[1,768,2048]{2,1,0:T(8,128)(2,1)S(1)}, bf16[384,512]{1,0:T...) custom-call(s32[2,128]{1,0:T(2,128)} %bitcast.5, ...), custom_call_target="tpu_custom_call" | custom-call | tf_op jit(solution)/shard_map/layer/pallas_call | solution.py:747
  47.0 0.0 copy-done
  47.0 3.9 %finish.1 = (bf16[1,2048,768]{2,1,0:T(8,128)(2,1)}, bf16[1,2048,768]{2,1,0:T(8,128)(2,1)}, bf16[1,768,2048]{2,1,0:T(8,128)(2,1)}, f32[128,512]{1,0:T(8,128)}, f3...) custom-call(bf16[1,2048,768]{2,1,0:T(8,128)(2,1)S(1)} %get-tuple-element.28., ...), custom_call_target="tpu_custom_call" | custom-call | tf_op jit(solution)/shard_map/finish/pallas_call | solution.py:897
Async XLA Ops:
  0.6 46.4 %copy-start = (bf16[2048,8]{0,1:T(8,128)(2,1)S(1)}, bf16[2048,8]{0,1:T(8,128)(2,1)}, u32[]{:S(2)}) copy-start(bf16[2048,8]{0,1:T(8,128)(2,1)} %param.15) | copy-start | bytes 98308
